TPU v7x, 512 devices: a whole 4x4x16 slice. The times are simulated.
512 devices in a mesh: ep: 128 (over z, x, core), tp: 4 (over y).
Axes of the slice: x: 4, y: 4, z: 16, core: 2. Of those that a mesh axis runs over, the one named last changes fastest.
Arguments:
- residual_in: bfloat16 [1920, 1536], P('ep'), may hold values from -6 to 6
- rec_state: bfloat16 [1920, 12, 128, 128], P('ep', 'tp'), may hold values from -6 to 6
- mix_gain: float32 [1536], replicated, may hold values from 0.1 to 1.9
- w_query: bfloat16 [1536, 1536], P('tp', 'ep'), may hold values from -0.15625 to 0.15625
- w_forget: bfloat16 [1536, 1536], P('tp', 'ep'), may hold values from -0.15625 to 0.15625
- w_input: bfloat16 [1536, 1536], P('tp', 'ep'), may hold values from -0.15625 to 0.15625
- w_gate: bfloat16 [1536, 1536], P('tp', 'ep'), may hold values from -0.15625 to 0.15625
- lower_bound: float32 [1536], P('tp'), may hold values from 0 to 0.9
- head_gain: float32 [128], replicated, may hold values from 0.1 to 1.9
- w_out: bfloat16 [1536, 1536], P('tp', 'ep'), may hold values from -0.15625 to 0.15625
- ffn_gain: float32 [1536], replicated, may hold values from 0.1 to 1.9
- route_ids: int32 [1920, 6], P('ep'), may hold values from 0 to 127, all different within a row; in each aligned block of 15 rows (0 to 14, 15 to 29, ...) at most 2 rows name the same one
- route_weight: float32 [1920, 6], P('ep'), may hold values from 0.2 to 1
- expert_gate: bfloat16 [128, 1536, 512], P('ep', None, 'tp'), may hold values from -0.15625 to 0.15625
- expert_up: bfloat16 [128, 1536, 512], P('ep', None, 'tp'), may hold values from -0.15625 to 0.15625
- expert_down: bfloat16 [128, 512, 1536], P('ep', 'tp'), may hold values from -0.25 to 0.25
Outputs:
- layer_out: bfloat16 [1920, 1536], P('ep', 'tp')
- new_state: bfloat16 [1920, 12, 128, 128], P('ep', 'tp')
Inputs may be any that keep to these rules, and one draw needn't show every extreme that they name: `route_ids`: each row names 6 different experts. Among the rows of one device no expert is named more than 2 times, and in every draw some device names some expert exactly 2 times.
All inputs are finite; a program needn't handle non-finite values.
Results may differ from a plain program's by a relative error of at most 0.016.
Values may be sent and summed in bfloat16 or wider, within the bound.
A program may use at most 64 MiB of HBM per device.

v0:
```python
import jax
import jax.numpy as jnp
from jax import lax
from jax.sharding import Mesh
from jax.sharding import PartitionSpec as P

EP = ("ep_0", "ep_1", "ep_2")


rms_eps = 1e-06


def in_order(pieces, dim):
    pieces = jnp.moveaxis(pieces, 0, dim)
    shape = pieces.shape
    return pieces.reshape(*shape[:dim], shape[dim] * shape[dim + 1], *shape[dim + 2 :])


def gather_in_order(x, axes, turns):
    pieces = x[None]
    for k in turns:
        pieces = lax.all_gather(pieces, axes[k], axis=0, tiled=True)
    carried = [lax.axis_size(axes[k]) for k in reversed(turns)]
    pieces = pieces.reshape(*carried, *x.shape)
    turned = sorted(range(len(turns)), key=lambda place: turns[len(turns) - 1 - place])
    return pieces.transpose(*turned, *range(len(turns), pieces.ndim)).reshape(-1, *x.shape)


def gather_axes(x, axes, turns, dim):
    return in_order(gather_in_order(x, axes, turns), dim)


def split_up(x, dim, count):
    shape = x.shape
    pieces = x.reshape(*shape[:dim], count, shape[dim] // count, *shape[dim + 1 :])
    return jnp.moveaxis(pieces, dim, 0)


def sent_and_summed(x, axis, dim):
    pieces = split_up(x, dim, lax.axis_size(axis))
    arrived = lax.all_to_all(pieces, axis, split_axis=0, concat_axis=0, tiled=True)
    return arrived.sum(axis=0)


def rms_scale(values, gain):
    return values * lax.rsqrt(jnp.mean(values * values, axis=-1, keepdims=True) + rms_eps) * gain


def rounded(values):
    return lax.optimization_barrier(values.astype(jnp.bfloat16)).astype(jnp.float32)


def recurrence(lower_bound, head_gain, state_block, query_raw, forget_raw, input_raw, gate_raw):
    seq_count = state_block.shape[0]
    heads_local = state_block.shape[1]
    head_size = state_block.shape[2]
    head_shape = (seq_count, heads_local, head_size)
    forget = lower_bound + (1.0 - lower_bound) * jax.nn.sigmoid(forget_raw)
    query_act = jax.nn.silu(query_raw).reshape(head_shape)
    key_act = (1.0 - forget).reshape(head_shape)
    forget_heads = forget.reshape(head_shape)
    value_act = input_raw.reshape(head_shape)
    state_next = (
        forget_heads[:, :, :, None] * state_block.astype(jnp.float32)
        + key_act[:, :, :, None] * value_act[:, :, None, :]
    )
    readout = jnp.einsum("shk,shkv->shv", query_act, state_next, precision=lax.Precision.HIGHEST)
    gate_heads = jax.nn.silu(gate_raw).reshape(head_shape)
    heads_out = rms_scale(readout, head_gain) * gate_heads
    return (
        state_next.astype(jnp.bfloat16),
        heads_out.reshape(seq_count, heads_local * head_size).astype(jnp.bfloat16),
    )


def shards(
    residual_in,
    rec_state,
    mix_gain,
    w_query,
    w_forget,
    w_input,
    w_gate,
    lower_bound,
    head_gain,
    w_out,
    ffn_gain,
    route_ids,
    route_weight,
    expert_gate,
    expert_up,
    expert_down,
):
    tp_count = lax.axis_size("tp")
    tp_rank = lax.axis_index("tp")
    ep_count = lax.axis_size(EP)
    seq_count = residual_in.shape[0]
    model_width = residual_in.shape[1]
    quarter = model_width // tp_count
    residual = residual_in.astype(jnp.float32)
    normed = rms_scale(residual, mix_gain).astype(jnp.bfloat16)
    own_rows = lax.dynamic_slice_in_dim(normed, tp_rank * quarter, quarter, 1)
    rows_piece = gather_axes(own_rows, EP, (0, 1, 2), 0)
    partial_proj = jnp.stack(
        [
            jnp.dot(rows_piece, weight, preferred_element_type=jnp.float32)
            for weight in (w_query, w_forget, w_input, w_gate)
        ],
        axis=1,
    )
    arrived = lax.all_to_all(
        partial_proj.astype(jnp.bfloat16), EP, split_axis=0, concat_axis=2, tiled=True
    ).astype(partial_proj.dtype)
    summed = sent_and_summed(arrived, "tp", 2)
    projected = rounded(summed)
    new_state, heads_out = recurrence(
        lower_bound,
        head_gain,
        rec_state,
        projected[:, 0],
        projected[:, 1],
        projected[:, 2],
        projected[:, 3],
    )
    partial_mix = jnp.dot(
        gather_axes(heads_out, EP, (0, 1, 2), 0), w_out, preferred_element_type=jnp.float32
    )
    mixed_home = lax.all_to_all(
        partial_mix.astype(jnp.bfloat16), EP, split_axis=0, concat_axis=1, tiled=True
    ).astype(partial_mix.dtype)
    mixed = lax.psum(mixed_home.astype(jnp.bfloat16), "tp").astype(jnp.float32)
    after_mix = rounded(residual + mixed)
    normed_ffn = rms_scale(after_mix, ffn_gain).astype(jnp.bfloat16)
    exp_dev = expert_gate.shape[0]
    experts_all = ep_count * exp_dev
    top_count = route_ids.shape[1]
    capacity = max(2, seq_count * top_count // experts_all + 1)
    flat_ids = route_ids.reshape(-1)
    onehot = (flat_ids[:, None] == jnp.arange(experts_all, dtype=jnp.int32)[None, :]).astype(
        jnp.int32
    )
    slot_rank = jnp.sum(jnp.cumsum(onehot, axis=0) * onehot, axis=1) - 1
    slot_index = flat_ids * capacity + slot_rank
    placer_int = (
        jnp.arange(experts_all * capacity, dtype=jnp.int32)[:, None] == slot_index[None, :]
    ).astype(jnp.int32)
    placer = jnp.sum(
        placer_int.reshape(experts_all * capacity, seq_count, top_count), axis=2
    ).astype(jnp.bfloat16)
    buffer = (
        jnp.dot(placer, normed_ffn, preferred_element_type=jnp.float32)
        .astype(jnp.bfloat16)
        .reshape(experts_all, capacity, model_width)
    )
    down_quarter = lax.all_to_all(expert_down, "tp", split_axis=2, concat_axis=1, tiled=True)
    own_quarter = lax.dynamic_slice_in_dim(buffer, tp_rank * quarter, quarter, 2)
    received = lax.all_gather(
        lax.all_to_all(own_quarter, EP, split_axis=0, concat_axis=0, tiled=True),
        "tp",
        axis=2,
        tiled=True,
    )
    slot_count = received.shape[1]
    grouped = received.reshape(ep_count, exp_dev, slot_count, model_width)
    gate_part = jnp.einsum(
        "sjnd,jdf->sjnf", grouped, expert_gate, preferred_element_type=jnp.float32
    )
    up_part = jnp.einsum("sjnd,jdf->sjnf", grouped, expert_up, preferred_element_type=jnp.float32)
    hidden = (jax.nn.silu(gate_part) * up_part).astype(jnp.bfloat16)
    hidden_whole = lax.all_gather(hidden, "tp", axis=3, tiled=True)
    summed_down = jnp.einsum(
        "sjnf,jfd->sjnd", hidden_whole, down_quarter, preferred_element_type=jnp.float32
    )
    returned = summed_down.astype(jnp.bfloat16).reshape(experts_all, slot_count, quarter)
    gathered_back = lax.all_to_all(returned, EP, split_axis=0, concat_axis=0, tiled=True)
    flat_back = gathered_back.reshape(experts_all * capacity, quarter)
    picked = (
        jnp.take(flat_back, slot_index, axis=0)
        .astype(jnp.float32)
        .reshape(seq_count, top_count, quarter)
    )
    expert_sum = jnp.sum(route_weight[:, :, None] * picked, axis=1)
    own_mix = lax.dynamic_slice_in_dim(after_mix, tp_rank * quarter, quarter, 1)
    layer_out = (own_mix + expert_sum).astype(jnp.bfloat16)
    return (layer_out, new_state)


def solution(mesh):
    split = Mesh(mesh.devices.reshape(16, 4, 2, mesh.shape["tp"]), ("ep_0", "ep_1", "ep_2", "tp"))
    in_specs = (
        P(EP, None),
        P(EP, "tp", None, None),
        P(),
        P("tp", EP),
        P("tp", EP),
        P("tp", EP),
        P("tp", EP),
        P("tp"),
        P(),
        P("tp", EP),
        P(),
        P(EP, None),
        P(EP, None),
        P(EP, None, "tp"),
        P(EP, None, "tp"),
        P(EP, "tp", None),
    )
    out_specs = (P(EP, "tp"), P(EP, "tp", None, None))
    return jax.shard_map(
        shards, mesh=split, in_specs=in_specs, out_specs=out_specs, check_vma=False
    )
```

profile of v0, /device:TPU:1, one launch (start us, length us, event | category | flops | bytes accessed | tf_op | source)
XLA Modules:
  0.0 379.0 jit_solution(7095298848502232704)
XLA Ops:
  7.2 0.8 convert_element_type.89
  8.1 0.9 multiply_reduce_fusion.2
  9.0 0.8 dynamic-slice
  9.9 30.2 %all-gather.1 = bf16[16,15,384]{2,1,0:T(8,128)(2,1)S(1)} all-gather(bf16[1,15,384]{2,1,0:T(8,128)(2,1)S(1)} %fusion.28), channel_id=2, replica_groups=mesh['ep_0'=16,'ep_1'=4,'ep_2'=2,'tp'=4] {'ep_0'}, dimensions={0}, use_global_device_ids=true | all-gather | bytes 195840 | tf_op jit(solution)/shard_map/all_gather | solution.py:22
  40.1 11.6 %all_gather.25 = bf16[64,15,384]{2,0,1:T(8,128)(2,1)} all-gather(bf16[16,15,384]{2,0,1:T(8,128)(2,1)S(1)} %copy.112), channel_id=1, replica_groups=mesh['ep_0'=16,'ep_1'=4,'ep_2'=2,'tp'=4] {'ep_1'}, dimensions={0}, use_global_device_ids=true | all-gather | bytes 921600 | tf_op jit(solution)/shard_map/all_gather | solution.py:22
  51.7 26.9 %all-gather.5.cloned.1.call-done = bf16[128,15,384]{2,0,1:T(8,128)(2,1)} async-done(((bf16[64,15,384]{2,0,1:T(8,128)(2,1)}), bf16[128,15,384]{2,0,1:T(8,128)(2,1)}) %all-gather.5.cloned.1.call-update) | async-done | bytes 1474576 | tf_op jit(solution)/shard_map/all_gather | solution.py:22
  78.6 2.2 copy.113
  80.8 0.5 reshape_reshape.6
  81.4 0.2 copy-done.5
  81.5 0.5 fusion.2
  82.0 0.2 copy-done.6
  82.3 0.5 fusion.3
  82.7 0.5 fusion.4
  83.3 0.5 fusion.5
  83.9 1.3 copy.114
  85.2 2.1 reshape.247
  87.3 33.0 %all_to_all.58 = bf16[128,2,360]{2,1,0:T(2,128)(2,1)S(1)} all-to-all(bf16[128,2,360]{2,1,0:T(2,128)(2,1)S(1)} %reshape.247), channel_id=1, replica_groups=mesh['ep_0'=16,'ep_1'=4,'ep_2'=2,'tp'=4] {'ep_0','ep_1','ep_2'}, dimensions={0} | all-to-all | bytes 368640 | tf_op jit(solution)/shard_map/all_to_all | solution.py:111
  120.4 1.1 reshape.248
  121.5 2.0 copy.115
  123.5 4.1 %reshape.222 = f32[128,15,4,12]{1,0,2,3:T(8,128)S(1)} reshape(bf16[1920,4,12]{0,1,2:T(4,128)(2,1)} %copy.115) | data formatting | bytes 552960 | tf_op jit(solution)/shard_map/transpose | solution.py:36
  127.6 6.1 %copy.116 = f32[15,4,128,12]{3,2,1,0:T(8,128)} copy(f32[15,4,128,12]{0,2,1,3:T(8,128)S(1)} %bitcast.98) | data formatting | bytes 737280 | tf_op jit(solution)/shard_map/transpose | solution.py:36
  133.7 4.8 %reshape.221 = f32[15,4,4,384]{3,2,1,0:T(4,128)S(1)} reshape(f32[15,4,128,12]{3,2,1,0:T(8,128)} %copy.116) | data formatting | bytes 737280 | tf_op jit(solution)/shard_map/transpose | solution.py:36
  138.6 0.8 copy.117
  139.4 4.0 %all-to-all-start.1 = ((f32[4,15,4,384]{3,2,1,0:T(4,128)}), f32[4,15,4,384]{3,2,1,0:T(4,128)S(1)}, u32[]{:S(2)}, u32[]{:S(2)}) async-start(f32[4,15,4,384]{3,2,1,0:T(4,128)} %copy.117), calls=%async_computation.1 | async-start | bytes 737280 | tf_op jit(solution)/shard_map/all_to_all | solution.py:41
  143.4 6.9 %all-to-all-done.1 = f32[4,15,4,384]{3,2,1,0:T(4,128)S(1)} async-done(((f32[4,15,4,384]{3,2,1,0:T(4,128)}), f32[4,15,4,384]{3,2,1,0:T(4,128)S(1)}, u32[]{:S(2)}, u32[]{:S(2)}) %all-to-all-start.1) | async-done | bytes 368672 | tf_op jit(solution)/shard_map/all_to_all | solution.py:41
  150.4 0.3 slice_reduce_fusion.2
  150.8 4.0 %fusion.1 = f32[15,3,1,128]{3,2,1,0:T(1,128)S(1)} fusion(bf16[15,3,128,128]{3,2,1,0:T(8,128)(2,1)S(1)} %copy-done.1, f32[15,3,128]{2,1,0:T(4,128)S(1)} %mul.168, f32[15,3,128]{2,1,0:T(4,128)S(1)} %get-tuple-element.8, f32[15,3,128]{2,1,0:T(4,128)S(1)} %get-tuple-element.9, f32[15,3,128,1]{2,1,0,3:T(4,128)S(1)} %fusion.21), kind=kOutput, calls=%fused_computation.3 | convolution fusion | flops 11796480 | bytes 1589760 | tf_op jit(solution)/shard_map/shk,shkv->shv/dot_general | solution.py:67
  155.1 23.5 %all_gather.27 = bf16[16,15,384]{2,1,0:T(8,128)(2,1)S(1)} all-gather(bf16[1,15,384]{2,1,0:T(8,128)(2,1)S(1)} %convert_element_type.98), channel_id=1, replica_groups=mesh['ep_0'=16,'ep_1'=4,'ep_2'=2,'tp'=4] {'ep_0'}, dimensions={0}, use_global_device_ids=true | all-gather | bytes 195840 | tf_op jit(solution)/shard_map/all_gather | solution.py:22
  178.6 11.3 %all_gather.28 = bf16[64,15,384]{2,0,1:T(8,128)(2,1)} all-gather(bf16[16,15,384]{2,0,1:T(8,128)(2,1)S(1)} %copy.119), channel_id=1, replica_groups=mesh['ep_0'=16,'ep_1'=4,'ep_2'=2,'tp'=4] {'ep_1'}, dimensions={0}, use_global_device_ids=true | all-gather | bytes 921600 | tf_op jit(solution)/shard_map/all_gather | solution.py:22
  190.3 0.2 select_reduce_fusion
  190.5 22.1 %all-gather.7.cloned.1.call-done = bf16[128,15,384]{2,0,1:T(8,128)(2,1)} async-done(((bf16[64,15,384]{2,0,1:T(8,128)(2,1)}), bf16[128,15,384]{2,0,1:T(8,128)(2,1)}) %all-gather.7.cloned.1.call-update) | async-done | bytes 1474576 | tf_op jit(solution)/shard_map/all_gather | solution.py:22
  212.6 2.2 copy.149
  214.9 0.5 reshape_reshape.7
  215.4 1.2 convolution_convert_fusion.1
  216.6 0.8 all_to_all.43
  217.4 1.1 copy.121
  218.4 15.2 %all-to-all-start.2 = ((bf16[128,15,12]{1,2,0:T(8,128)(2,1)}), bf16[128,15,12]{1,2,0:T(8,128)(2,1)S(1)}, u32[]{:S(2)}, u32[]{:S(2)}) async-start(bf16[128,15,12]{1,2,0:T(8,128)(2,1)} %copy.121), calls=%async_computation.2 | async-start | bytes 1048576 | tf_op jit(solution)/shard_map/all_to_all | solution.py:128
  233.7 0.6 copy.128
  234.3 0.5 broadcast.193
  234.8 8.8 %reduce.8 = bf16[1536,128]{1,0:T(8,128)(2,1)S(1)} reduce(bf16[1536,1,128]{2,1,0:T(2,128)(2,1)S(1)} %bitcast.100, bf16[]{:T(256)} %broadcast.193), dimensions={1}, to_apply=%bitcast.82.reduce_sub_computation | reduce | bytes 786434
  243.6 0.8 reshape.245
  244.6 19.7 %all-to-all-done.2 = bf16[128,15,12]{1,2,0:T(8,128)(2,1)S(1)} async-done(((bf16[128,15,12]{1,2,0:T(8,128)(2,1)}), bf16[128,15,12]{1,2,0:T(8,128)(2,1)S(1)}, u32[]{:S(2)}, u32[]{:S(2)}) %all-to-all-start.2) | async-done | bytes 46112 | tf_op jit(solution)/shard_map/all_to_all | solution.py:128
  264.3 4.0 %all-to-all-start.4 = ((bf16[4,2,24576]{2,1,0:T(2,128)(2,1)}), bf16[4,2,24576]{2,1,0:T(2,128)(2,1)S(1)}, u32[]{:S(2)}, u32[]{:S(2)}) async-start(bf16[4,2,24576]{2,1,0:T(2,128)(2,1)} %reshape.245), calls=%async_computation.4 | async-start | bytes 786432 | tf_op jit(solution)/shard_map/all_to_all | solution.py:155
  268.3 0.2 reshape.240
  268.5 0.2 copy.133
  268.7 13.8 %psum.7 = bf16[15,1536]{1,0:T(8,128)(2,1)S(1)} all-reduce(bf16[15,1536]{1,0:T(8,128)(2,1)S(1)} %copy.133), channel_id=1, replica_groups=mesh['ep_0'=16,'ep_1'=4,'ep_2'=2,'tp'=4] {'tp'}, use_global_device_ids=true, to_apply=%region_3.4 | all-reduce | flops 23040 | bytes 92160 | tf_op jit(solution)/shard_map/psum | solution.py:131
  282.7 0.4 convolution_convert_fusion
  283.1 0.3 reshape.215
  283.4 0.8 constant_dynamic-slice_fusion
  284.2 13.5 %all-to-all-start.3 = ((bf16[128,2,384]{2,1,0:T(2,128)(2,1)}), bf16[128,2,384]{2,1,0:T(2,128)(2,1)S(1)}, u32[]{:S(2)}, u32[]{:S(2)}) async-start(bf16[128,2,384]{2,1,0:T(2,128)(2,1)} %constant_dynamic-slice_fusion), calls=%async_computation.3 | async-start | bytes 393216 | tf_op jit(solution)/shard_map/all_to_all | solution.py:158
  297.8 0.4 reshape.246
  298.2 0.2 copy.129
  298.5 17.3 %all-to-all-done.3 = bf16[128,2,384]{2,1,0:T(2,128)(2,1)S(1)} async-done(((bf16[128,2,384]{2,1,0:T(2,128)(2,1)}), bf16[128,2,384]{2,1,0:T(2,128)(2,1)S(1)}, u32[]{:S(2)}, u32[]{:S(2)}) %all-to-all-start.3) | async-done | bytes 196640 | tf_op jit(solution)/shard_map/all_to_all | solution.py:158
  315.8 11.9 %all_gather.30 = bf16[128,2,1536]{2,0,1:T(8,128)(2,1)S(1)} all-gather(bf16[128,2,384]{2,0,1:T(8,128)(2,1)S(1)} %copy.127), channel_id=1, replica_groups=mesh['ep_0'=16,'ep_1'=4,'ep_2'=2,'tp'=4] {'tp'}, dimensions={2}, use_global_device_ids=true | all-gather | bytes 983040 | tf_op jit(solution)/shard_map/all_gather | solution.py:157
  327.7 0.4 convolution_bitcast_fusion.1
  328.1 0.4 fusion.10
  328.5 10.0 %all_gather.31 = bf16[128,1,2,512]{3,0,2,1:T(8,128)(2,1)S(1)} all-gather(bf16[128,1,2,128]{3,0,2,1:T(8,128)(2,1)S(1)} %fusion.10), channel_id=1, replica_groups=mesh['ep_0'=16,'ep_1'=4,'ep_2'=2,'tp'=4] {'tp'}, dimensions={3}, use_global_device_ids=true | all-gather | bytes 327680 | tf_op jit(solution)/shard_map/all_gather | solution.py:170
  338.5 0.3 convolution_convert_fusion.6
  338.8 0.9 copy.130
  339.7 12.8 %all-to-all-start.5 = ((bf16[128,2,384]{2,1,0:T(2,128)(2,1)}), bf16[128,2,384]{2,1,0:T(2,128)(2,1)S(1)}, u32[]{:S(2)}, u32[]{:S(2)}) async-start(bf16[128,2,384]{2,1,0:T(2,128)(2,1)} %copy.130), calls=%async_computation.5 | async-start | bytes 393216 | tf_op jit(solution)/shard_map/all_to_all | solution.py:175
  352.7 2.9 fusion
  355.6 14.9 %all-to-all-done.5 = bf16[128,2,384]{2,1,0:T(2,128)(2,1)S(1)} async-done(((bf16[128,2,384]{2,1,0:T(2,128)(2,1)}), bf16[128,2,384]{2,1,0:T(2,128)(2,1)S(1)}, u32[]{:S(2)}, u32[]{:S(2)}) %all-to-all-start.5) | async-done | bytes 196640 | tf_op jit(solution)/shard_map/all_to_all | solution.py:175
  370.6 0.8 gather_fusion
  371.6 0.6 add_convert_fusion.1
  (78 shorter events, 2.1 us)
Async XLA Ops:
  7.2 320.5 %copy-start = (bf16[1,1536,128]{2,1,0:T(8,128)(2,1)S(1)}, bf16[1,1536,128]{2,1,0:T(8,128)(2,1)}, u32[]{:S(2)}) copy-start(bf16[1,1536,128]{2,1,0:T(8,128)(2,1)} %param.29) | copy-start | bytes 1179652
  7.2 71.4 %all-gather.5.cloned.1.call-start = ((), (), s32[]{:S(2)}) async-start(), calls=%async_computation.6 | async-start | bytes 2211840 | tf_op jit(solution)/shard_map/all_gather | solution.py:22
  80.8 0.7 copy-start.5
  81.5 0.7 copy-start.6
  81.5 1.2 copy-start.7
  82.3 1.0 copy-start.8
  133.7 9.7 %copy-start.10 = (f32[384]{0:T(512)S(1)}, f32[384]{0:T(512)}, u32[]{:S(2)}) copy-start(f32[384]{0:T(512)} %param.23) | copy-start | bytes 4612
  138.5 12.3 %copy-start.1 = (bf16[15,3,128,128]{3,2,1,0:T(8,128)(2,1)S(1)}, bf16[15,3,128,128]{3,2,1,0:T(8,128)(2,1)}, u32[]{:S(2)}) copy-start(bf16[15,3,128,128]{3,2,1,0:T(8,128)(2,1)} %param.17) | copy-start | bytes 4423684
  139.4 10.9 %all-to-all-start.1 = ((f32[4,15,4,384]{3,2,1,0:T(4,128)}), f32[4,15,4,384]{3,2,1,0:T(4,128)S(1)}, u32[]{:S(2)}, u32[]{:S(2)}) async-start(f32[4,15,4,384]{3,2,1,0:T(4,128)} %copy.117), calls=%async_computation.1 | async-start | bytes 737280 | tf_op jit(solution)/shard_map/all_to_all | solution.py:41
  143.4 69.2 %all-gather.7.cloned.1.call-start = ((), (), s32[]{:S(2)}) async-start(), calls=%async_computation.7 | async-start | bytes 2211840 | tf_op jit(solution)/shard_map/all_gather | solution.py:22
  150.8 4.1 %copy-start.13 = (f32[128]{0:T(128)S(1)}, f32[128]{0:T(128)}, u32[]{:S(2)}) copy-start(f32[128]{0:T(128)} %param.24) | copy-start | bytes 1540
  154.8 35.0 %copy-start.11 = (s32[15,6]{0,1:T(8,128)S(1)}, s32[15,6]{0,1:T(8,128)}, u32[]{:S(2)}) copy-start(s32[15,6]{0,1:T(8,128)} %param.27) | copy-start | bytes 1084
  190.4 22.2 %copy-start.14 = (s32[90]{0:T(128)}, s32[90]{0:T(128)S(1)}, u32[]{:S(2)}) copy-start(s32[90]{0:T(128)S(1)} %select_reduce_fusion) | copy-start | bytes 1084
  216.6 17.1 %copy-start.4 = (bf16[1,128,1536]{2,1,0:T(8,128)(2,1)S(1)}, bf16[1,128,1536]{2,1,0:T(8,128)(2,1)}, u32[]{:S(2)}) copy-start(bf16[1,128,1536]{2,1,0:T(8,128)(2,1)} %param.31) | copy-start | bytes 1179652
  218.4 45.8 %all-to-all-start.2 = ((bf16[128,15,12]{1,2,0:T(8,128)(2,1)}), bf16[128,15,12]{1,2,0:T(8,128)(2,1)S(1)}, u32[]{:S(2)}, u32[]{:S(2)}) async-start(bf16[128,15,12]{1,2,0:T(8,128)(2,1)} %copy.121), calls=%async_computation.2 | async-start | bytes 1048576 | tf_op jit(solution)/shard_map/all_to_all | solution.py:128
  243.6 38.9 %copy-start.3 = (bf16[15,1536]{1,0:T(8,128)(2,1)S(1)}, bf16[15,1536]{1,0:T(8,128)(2,1)}, u32[]{:S(2)}) copy-start(bf16[15,1536]{1,0:T(8,128)(2,1)} %param.16) | copy-start | bytes 138244
  243.6 39.0 %copy-start.9 = (f32[1536]{0:T(1024)S(1)}, f32[1536]{0:T(1024)}, u32[]{:S(2)}) copy-start(f32[1536]{0:T(1024)} %param.26) | copy-start | bytes 18436
  264.3 19.9 %all-to-all-start.4 = ((bf16[4,2,24576]{2,1,0:T(2,128)(2,1)}), bf16[4,2,24576]{2,1,0:T(2,128)(2,1)S(1)}, u32[]{:S(2)}, u32[]{:S(2)}) async-start(bf16[4,2,24576]{2,1,0:T(2,128)(2,1)} %reshape.245), calls=%async_computation.4 | async-start | bytes 786432 | tf_op jit(solution)/shard_map/all_to_all | solution.py:155
  284.2 31.6 %all-to-all-start.3 = ((bf16[128,2,384]{2,1,0:T(2,128)(2,1)}), bf16[128,2,384]{2,1,0:T(2,128)(2,1)S(1)}, u32[]{:S(2)}, u32[]{:S(2)}) async-start(bf16[128,2,384]{2,1,0:T(2,128)(2,1)} %constant_dynamic-slice_fusion), calls=%async_computation.3 | async-start | bytes 393216 | tf_op jit(solution)/shard_map/all_to_all | solution.py:158
  298.5 29.6 %copy-start.16 = (bf16[1,1536,128]{2,1,0:T(8,128)(2,1)S(1)}, bf16[1,1536,128]{2,1,0:T(8,128)(2,1)}, u32[]{:S(2)}) copy-start(bf16[1,1536,128]{2,1,0:T(8,128)(2,1)} %param.30) | copy-start | bytes 1179652
  328.1 24.5 %copy-start.12 = (f32[15,6]{0,1:T(8,128)S(1)}, f32[15,6]{0,1:T(8,128)}, u32[]{:S(2)}) copy-start(f32[15,6]{0,1:T(8,128)} %param.28) | copy-start | bytes 1084
  328.1 24.6 %copy-start.15 = (s32[90]{0:T(128)S(1)}, s32[90]{0:T(128)}, u32[]{:S(2)}) copy-start(s32[90]{0:T(128)} %copy-done.14) | copy-start | bytes 1084
  328.1 24.6 %copy-start.2 = (bf16[15,3,128,128]{3,2,1,0:T(8,128)(2,1)S(1)}, bf16[15,3,128,128]{3,2,1,0:T(8,128)(2,1)}, u32[]{:S(2)}) copy-start(bf16[15,3,128,128]{3,2,1,0:T(8,128)(2,1)} %param.17) | copy-start | bytes 4423684
  339.7 30.9 %all-to-all-start.5 = ((bf16[128,2,384]{2,1,0:T(2,128)(2,1)}), bf16[128,2,384]{2,1,0:T(2,128)(2,1)S(1)}, u32[]{:S(2)}, u32[]{:S(2)}) async-start(bf16[128,2,384]{2,1,0:T(2,128)(2,1)} %copy.130), calls=%async_computation.5 | async-start | bytes 393216 | tf_op jit(solution)/shard_map/all_to_all | solution.py:175
Sparse Core Ops, SparseCore 0:
  51.8 26.7 all-gather.4
  190.0 22.6 all-gather.6
where the time goes:
time: 381 us; the launch traced here: 379 us
  blocking collectives  145 us (38%)
  waiting for transfers between devices  108 us (28%)
  starting transfers between devices  49.6 us (13%)
  local copies, waits for them, and re-layouts  37.6 us (10%)
  other arithmetic  15.6 us (4%)
  between operations  14.5 us (4%)
  matrix products  8.61 us (2%)
    all_gather x4, blocking collectives, gather_in_order(): pieces = lax.all_gather(pieces, axes[k], axis=0, tiled=True)  76.4 us
    all_gather x2, waiting for transfers between devices, gather_in_order(): pieces = lax.all_gather(pieces, axes[k], axis=0, tiled=True)  49 us
    all_to_all x1, blocking collectives, shards(): lax.all_to_all(partial_proj.astype(jnp.bfloat16), EP, split_axis=0, conca...  33 us
    all_to_all x1, waiting for transfers between devices, shards(): lax.all_to_all(partial_mix.astype(jnp.bfloat16), EP, split_axis=0, concat...  19.7 us
    all_to_all x1, waiting for transfers between devices, shards(): lax.all_to_all(own_quarter, EP, split_axis=0, concat_axis=0, tiled=True)  17.3 us
    transpose x4, local copies, waits for them, and re-layouts, split_up(): return jnp.moveaxis(pieces, dim, 0)  15.9 us
    all_to_all x1, starting transfers between devices, shards(): lax.all_to_all(partial_mix.astype(jnp.bfloat16), EP, split_axis=0, concat...  15.2 us
    all_to_all x1, waiting for transfers between devices, shards(): lax.all_to_all(returned, EP, split_axis=0, concat_axis=0, tiled=True)  14.9 us
  transfers between devices with their start and end apart: 7, of which 6 were waited for; matrix products, arithmetic and copies ran while one was open for 5% of the time, Pallas kernels for 0%

commit v1 on v0

v1 whole, which is shorter than its diff:
```python
import jax
import jax.numpy as jnp
from jax import lax
from jax.experimental import pallas as pl
from jax.experimental.pallas import tpu as pltpu
from jax.sharding import Mesh
from jax.sharding import PartitionSpec as P

EP = ("ep_0", "ep_1", "ep_2")
EPS = 1e-06
BF = jnp.bfloat16
F32 = jnp.float32
NZ, NX, NC, NY = 16, 4, 2, 4
XC = NX * NC
D, Q, SEQ, HEAD, HL, FQ, TOPK = 1536, 384, 15, 128, 3, 128, 6
COLS = 12


def dot(a, b):
    return lax.dot_general(a, b, (((1,), (0,)), ((), ())), preferred_element_type=F32)


def dot_t(a, b):
    return lax.dot_general(a, b, (((1,), (1,)), ((), ())), preferred_element_type=F32)


def iota(shape, dim):
    return lax.broadcasted_iota(jnp.int32, shape, dim)


def split_two(x):
    hi = x.astype(BF)
    return hi, (x - hi.astype(F32)).astype(BF)


def sigmoid(x):
    return 1.0 / (1.0 + jnp.exp(-x))


def kernel(
    res_ref,
    mix_gain_ref,
    w_ref,
    lower_ref,
    head_gain_ref,
    ffn_gain_ref,
    ids_ref,
    rw_ref,
    state_hbm,
    eg_hbm,
    eu_hbm,
    ed_hbm,
    out_ref,
    new_state_hbm,
    wz,
    wo,
    tok,
    psend,
    precv,
    perm_in,
    state_v,
    state_o,
    cols,
    rows_s,
    read_s,
    ho,
    rsend,
    rrecv,
    ssend,
    srecv,
    res_s,
    ids_s,
    rw_s,
    tz,
    xsend,
    xf,
    hf,
    dq,
    wg_v,
    wu_v,
    osend,
    orecv,
    zsend,
    zrecv,
    z1s,
    z1r,
    toks,
    tokr,
    ps,
    pr,
    wos,
    wor,
    rss,
    rsr,
    sss,
    ssr,
    z2s,
    z2r,
    xs,
    xr,
    ys,
    yr,
    hs,
    hr,
    ds_,
    dr,
    os_,
    or_,
    rets,
    retr,
    local,
):
    z = lax.axis_index("ep_0")
    x = lax.axis_index("ep_1")
    c = lax.axis_index("ep_2")
    y = lax.axis_index("tp")
    me = x * NC + c
    pending = []

    def dev(dz=0, dx=0, dc=0, dy=0):
        return {
            "ep_0": lax.rem(z + dz + NZ, NZ),
            "ep_1": lax.rem(x + dx + NX, NX),
            "ep_2": lax.rem(c + dc + NC, NC),
            "tp": lax.rem(y + dy + NY, NY),
        }

    def send(src, dst, ss, rs, to):
        copy = pltpu.make_async_remote_copy(
            src_ref=src,
            dst_ref=dst,
            send_sem=ss,
            recv_sem=rs,
            device_id=to,
            device_id_type=pl.DeviceIdType.MESH,
        )
        copy.start()
        pending.append(copy)

    def arrive(dst, ss, rs):
        pltpu.make_async_remote_copy(
            src_ref=dst,
            dst_ref=dst,
            send_sem=ss,
            recv_sem=rs,
            device_id=dev(),
            device_id_type=pl.DeviceIdType.MESH,
        ).wait_recv()

    def zi(d):
        return lax.rem(z + d + NZ, NZ)

    def yi(d):
        return lax.rem(y + d + NY, NY)

    groups = [(dx, dc) for dx in range(NX) for dc in range(NC)]

    def xc_to(g):
        return lax.rem(x + g[0], NX) * NC + lax.rem(c + g[1], NC)

    def xc_from(g):
        return lax.rem(x - g[0] + NX, NX) * NC + lax.rem(c - g[1] + NC, NC)

    loads = [
        pltpu.make_async_copy(state_hbm, state_v, local.at[0]),
        pltpu.make_async_copy(eg_hbm, wg_v, local.at[1]),
        pltpu.make_async_copy(eu_hbm, wu_v, local.at[2]),
    ]

    def quarter(ref, part):
        return ref.at[:, pl.ds(pl.multiple_of(part * Q, Q), Q)]

    own_down = pltpu.make_async_copy(quarter(ed_hbm, y), dq.at[y], local.at[3])

    barrier = pltpu.get_barrier_semaphore()
    peers = [dict(dz=d) for d in range(1, NZ)]
    for g in groups:
        for dy in range(NY):
            if g != (0, 0) or dy:
                peers.append(dict(dx=g[0], dc=g[1], dy=dy))
    for p in peers:
        pl.semaphore_signal(
            barrier, inc=1, device_id=dev(**p), device_id_type=pl.DeviceIdType.MESH
        )

    res_s[...] = jnp.zeros_like(res_s)
    res_s[0:SEQ, :] = res_ref[...].astype(F32)
    own_w = pltpu.make_async_copy(w_ref, wz.at[z], local.at[4])
    own_w.start()
    res = res_s[...]
    scale = lax.rsqrt(jnp.mean(res * res, axis=-1, keepdims=True) + EPS)
    own = pl.ds(pl.multiple_of(y * Q, Q), Q)
    tok[me] = (res_s[:, own] * scale * mix_gain_ref[:, own]).astype(BF)
    own_w.wait()
    pl.semaphore_wait(barrier, len(peers))

    def z_start(buf, ss, rs):
        for k, d in ((2, 4), (3, -4), (0, 1), (1, -1), (4, 2), (5, -2)):
            send(buf.at[z], buf.at[z], ss.at[k], rs.at[k], dev(dz=d))

    def z_finish(buf, ss, rs, first, second):
        def block(d, part=None):
            ref = buf.at[zi(d)]
            return ref if part is None else ref.at[part]

        def pass_on(k, d, to, part=None):
            send(block(d, part), block(d, part), ss.at[k], rs.at[k], dev(dz=to))

        def got(k, d, part=None):
            arrive(block(d, part), ss.at[k], rs.at[k])

        got(2, -4)
        pass_on(6, -4, 4, first)
        got(3, 4)
        pass_on(10, 4, -4, second)
        for k, d, to in ((7, -4, 1), (8, -4, -1), (9, -4, 2), (11, 4, 1), (12, 4, -1), (13, 4, -2)):
            pass_on(k, d, to)
        got(6, 8, first)
        got(10, 8, second)
        pass_on(14, 8, 1)
        pass_on(15, 8, -1)
        for k, d in (
            (0, -1), (1, 1), (4, -2), (5, 2), (7, -5), (8, -3),
            (9, -6), (11, 3), (12, 5), (13, 6), (14, 7), (15, 9),
        ):
            got(k, d)

    z_start(wz, z1s, z1r)
    for i, g in enumerate(groups[1:], 1):
        send(tok.at[me], tok.at[me], toks.at[i], tokr.at[i], dev(dx=g[0], dc=g[1]))
    for copy in loads:
        copy.start()
    own_down.start()
    for k in range(1, NY):
        send(quarter(ed_hbm, yi(k)), dq.at[y], ds_.at[k], dr.at[k], dev(dy=k))

    ids_s[...] = jnp.full_like(ids_s, -1)
    ids_s[0:SEQ, 0:TOPK] = ids_ref[...]
    rw_s[...] = jnp.zeros_like(rw_s)
    rw_s[0:SEQ, 0:TOPK] = rw_ref[...]
    ids, rw = ids_s[...], rw_s[...]
    lane = iota((16, 256), 1)
    expert, slot = lane // 2, lane % 2
    row = iota((16, 256), 0).astype(F32)
    named = jnp.zeros((16, 256), F32)
    weight = jnp.zeros((16, 256), F32)
    for j in range(TOPK):
        hit = ids[:, j : j + 1] == expert
        named = jnp.where(hit, 1.0, named)
        weight = jnp.where(hit, rw[:, j : j + 1], weight)
    low = jnp.min(jnp.where(named > 0.5, row, 99.0), axis=0, keepdims=True)
    high = jnp.max(jnp.where(named > 0.5, row, -1.0), axis=0, keepdims=True)
    second = jnp.where(high > low, high, 99.0)
    table = jnp.where(slot[0:1] == 0, low, second)
    combine = jnp.where(row == table, weight, 0.0)
    comb_hi, comb_lo = split_two(combine)

    k_id = iota((1024, 1), 0)
    k_xc, k_in = k_id // 128, k_id % 128
    k_q, k_pj = k_in // 64, k_in % 64
    k_p, k_j = k_pj // COLS, k_pj % COLS
    target = jnp.where(k_pj < 48, k_p * 256 + k_q * 96 + COLS * k_xc + k_j, -1)
    order_in = jnp.where(iota((1024, 1024), 1) == target, 1.0, 0.0).astype(BF)
    perm_in[...] = order_in

    z_finish(wz, z1s, z1r, (pl.ds(0, 32),), (pl.ds(32, 32),))

    wo_own = wz.at[:, pl.ds(48, 16), :]
    own_wo = pltpu.make_async_copy(wo_own, wo.at[me], local.at[5])
    own_wo.start()
    for i, g in enumerate(groups[1:], 1):
        arrive(tok.at[xc_from(g)], toks.at[i], tokr.at[i])
    tokens = tok[...].reshape(XC * 16, Q)

    pairs = [(g, dy) for dy in range(NY) for g in groups]
    for k in range(NY):
        part = yi(k)
        block = wz[pl.ds(4 * part, 4)].reshape(256, Q)
        psend[part] = dot_t(tokens, block).astype(BF).reshape(XC, 16, 256)
    precv[y, me] = psend[y, me]
    for i, (g, dy) in enumerate(pairs):
        if i == 0:
            continue
        send(
            psend.at[yi(dy), xc_to(g)],
            precv.at[y, me],
            ps.at[i],
            pr.at[i],
            dev(dx=g[0], dc=g[1], dy=dy),
        )
    for dx in range(1, NX):
        send(wo_own, wo.at[me], wos.at[dx], wor.at[dx], dev(dx=dx))
    send(wo_own, wo.at[me], wos.at[0], wor.at[0], dev(dc=1))

    for i, (g, dy) in enumerate(pairs):
        if i:
            arrive(precv.at[yi(-dy), xc_from(g)], ps.at[i], pr.at[i])
    halves = [[], []]
    for e in range(XC):
        total = precv[0, e].astype(F32)
        for k in range(1, NY):
            total = total + precv[k, e].astype(F32)
        total = total.astype(BF)
        halves[0].append(total[:, 0:128])
        halves[1].append(total[:, 128:256])
    stacked = jnp.concatenate(
        [jnp.concatenate(half, axis=1) for half in halves], axis=0
    )
    ordered = dot(stacked, perm_in[...])
    narrow = iota((16, 128), 1) < 64
    proj = []
    for p in range(4):
        a = ordered[0:16, 256 * p : 256 * p + 256]
        b = ordered[16:32, 256 * p : 256 * p + 256]
        b0 = pltpu.roll(b[:, 0:128], 64, 1)
        b1 = pltpu.roll(b[:, 128:256], 64, 1)
        proj.append(
            [a[:, 0:128], jnp.where(narrow, a[:, 128:256], b0), jnp.where(narrow, b0, b1)]
        )
    gates = []
    for h in range(HL):
        lower = lower_ref[:, h * HEAD : (h + 1) * HEAD]
        query = proj[0][h] * sigmoid(proj[0][h])
        forget = lower + (1.0 - lower) * sigmoid(proj[1][h])
        for n, values in enumerate((query, forget)):
            tall = jnp.concatenate([values, jnp.zeros((112, 128), F32)], axis=0)
            cols[n, h] = jnp.transpose(tall)
        rows_s[h] = proj[2][h]
        gates.append(proj[3][h] * sigmoid(proj[3][h]))

    loads[0].wait()
    read_s[...] = jnp.zeros_like(read_s)

    def one_head(h, _):
        queries, forgets, values = cols[0, h], cols[1, h], rows_s[h]
        for s in range(SEQ):
            f = forgets[:, s : s + 1]
            q = queries[:, s : s + 1]
            v = values[s : s + 1, :]
            nxt = f * state_v[s, h].astype(F32) + (1.0 - f) * v
            state_o[s, h] = nxt.astype(BF)
            read_s[h, s : s + 1, :] = jnp.sum(q * nxt, axis=0, keepdims=True)
        return 0

    lax.fori_loop(0, HL, one_head, 0)
    store = pltpu.make_async_copy(state_o, new_state_hbm, local.at[6])
    store.start()
    for h in range(HL):
        r = read_s[h]
        r = r * lax.rsqrt(jnp.mean(r * r, axis=-1, keepdims=True) + EPS)
        ho[:, h * HEAD : (h + 1) * HEAD] = (r * head_gain_ref[...] * gates[h]).astype(BF)

    for dx in range(1, NX):
        src = lax.rem(x - dx + NX, NX) * NC + c
        arrive(wo.at[src], wos.at[dx], wor.at[dx])
        send(wo.at[src], wo.at[src], wos.at[NX + dx], wor.at[NX + dx], dev(dc=1))
    other = 1 - c
    arrive(wo.at[x * NC + other], wos.at[0], wor.at[0])
    for dx in range(1, NX):
        src = lax.rem(x - dx + NX, NX) * NC + other
        arrive(wo.at[src], wos.at[NX + dx], wor.at[NX + dx])
    own_wo.wait()
    heads = ho[...]
    for k in (1, 2, 3, 0):
        part = yi(k)
        block = wo[:, pl.ds(4 * part, 4)].reshape(512, Q)
        rsend[part] = dot_t(heads, block).astype(BF)
        if k:
            send(rsend.at[part], rrecv.at[y], rss.at[k], rsr.at[k], dev(dy=k))
    rrecv[y] = rsend[y]
    o_id = iota((512, 1), 0)
    o_xc, o_q, o_j = o_id // 64, (o_id // 16) % 4, o_id % 16
    o_to = jnp.where(o_j < COLS, 96 * o_q + COLS * o_xc + o_j, -1)
    order_out = jnp.where(iota((512, Q), 1) == o_to, 1.0, 0.0).astype(BF)
    for k in range(1, NY):
        arrive(rrecv.at[yi(-k)], rss.at[k], rsr.at[k])
    total = rrecv[0].astype(F32)
    for k in range(1, NY):
        total = total + rrecv[k].astype(F32)
    both = dot(jnp.concatenate(split_two(total), axis=0), order_out)
    after = (res_s[:, own] + (both[0:16] + both[16:32])).astype(BF).astype(F32)
    square = jnp.sum(after * after, axis=-1, keepdims=True)
    ssend[...] = jnp.broadcast_to(square, (16, 128))
    srecv[y] = ssend[...]
    for k in range(1, NY):
        send(ssend, srecv.at[y], sss.at[k], ssr.at[k], dev(dy=k))
    gained = after * ffn_gain_ref[:, own]
    table_row = jnp.concatenate([table, jnp.zeros((1, 128), F32)], axis=1)
    is_table = iota((16, Q), 0) == SEQ
    for k in range(1, NY):
        arrive(srecv.at[yi(-k)], sss.at[k], ssr.at[k])
    square = srecv[0] + srecv[1] + srecv[2] + srecv[3]
    inverse = lax.rsqrt(square[:, 0:1] * (1.0 / D) + EPS)
    tz[z] = jnp.where(is_table, table_row, gained * inverse).astype(BF)

    z_start(tz, z2s, z2r)
    r_id, l_id = iota((256, 256), 0), iota((256, 256), 1)
    spread = jnp.where((r_id // 16 == l_id // 16) & (l_id % 16 == SEQ), 1.0, 0.0).astype(BF)
    mine = jnp.where(iota((16, 256), 1) == 16 * z + iota((16, 256), 0), 1.0, 0.0).astype(BF)
    same = iota((16, 256), 0) == iota((16, 256), 1) // 16
    token = (iota((16, 256), 1) % 16).astype(F32)
    loads[1].wait()
    loads[2].wait()
    z_finish(tz, z2s, z2r, (slice(None), pl.ds(0, 256)), (slice(None), pl.ds(256, 128)))
    flat = tz[...].reshape(256, Q)
    tables = dot(spread, flat[:, 0:256]).astype(BF)
    wanted = dot_t(mine, tables)
    hit = jnp.where(wanted == token, 1.0, 0.0)
    same_f = jnp.where(same, 1.0, 0.0)
    pick = (hit[:, None, :] * same_f[None, :, :]).reshape(256, 256).astype(BF)
    xsend[...] = dot(pick, flat).astype(BF).reshape(XC, 32, Q)
    xf[y, me] = xsend[me]
    for i, g in enumerate(groups[1:], 1):
        send(xsend.at[xc_to(g)], xf.at[y, me], xs.at[i], xr.at[i], dev(dx=g[0], dc=g[1]))
    for i, g in enumerate(groups):
        chunk = xf.at[y, xc_from(g)]
        if i:
            arrive(chunk, xs.at[i], xr.at[i])
        send(chunk, chunk, ys.at[0, i], yr.at[0, i], dev(dy=1))
        send(chunk, chunk, ys.at[1, i], yr.at[1, i], dev(dy=-1))

    def weights_of(part):
        at = pl.ds(pl.multiple_of(part * Q, Q), Q)
        return wg_v[at, :], wu_v[at, :]

    def add_part(part, sums):
        rows = xf[part].reshape(256, Q)
        a, b = weights_of(part)
        return sums[0] + dot(rows, a), sums[1] + dot(rows, b)

    sums = add_part(y, (jnp.zeros((256, FQ), F32), jnp.zeros((256, FQ), F32)))
    for i, g in enumerate(groups):
        left = xf.at[yi(-1), xc_from(g)]
        right = xf.at[yi(1), xc_from(g)]
        arrive(left, ys.at[0, i], yr.at[0, i])
        if i < 4:
            send(left, left, ys.at[2, i], yr.at[2, i], dev(dy=1))
        arrive(right, ys.at[1, i], yr.at[1, i])
        if i >= 4:
            send(right, right, ys.at[2, i], yr.at[2, i], dev(dy=-1))
    sums = add_part(yi(-1), sums)
    sums = add_part(yi(1), sums)
    for i, g in enumerate(groups):
        arrive(xf.at[yi(2), xc_from(g)], ys.at[2, i], yr.at[2, i])
    gate, up = add_part(yi(2), sums)
    hf[y] = (gate * sigmoid(gate) * up).astype(BF)

    send(hf.at[y], hf.at[y], hs.at[0], hr.at[0], dev(dy=1))
    send(hf.at[y], hf.at[y], hs.at[1], hr.at[1], dev(dy=-1))
    own_down.wait()
    for k in range(1, NY):
        arrive(dq.at[yi(-k)], ds_.at[k], dr.at[k])
    down = dot(hf[y], dq[y])
    top, bottom = pl.ds(0, 128), pl.ds(128, 128)
    left = hf.at[yi(-1)]
    right = hf.at[yi(1)]
    arrive(left, hs.at[0], hr.at[0])
    send(left.at[top], left.at[top], hs.at[2], hr.at[2], dev(dy=1))
    arrive(right, hs.at[1], hr.at[1])
    send(right.at[bottom], right.at[bottom], hs.at[3], hr.at[3], dev(dy=-1))
    down = down + dot(hf[yi(-1)], dq[yi(-1)]) + dot(hf[yi(1)], dq[yi(1)])
    far = hf.at[yi(2)]
    arrive(far.at[top], hs.at[2], hr.at[2])
    arrive(far.at[bottom], hs.at[3], hr.at[3])
    down = down + dot(hf[yi(2)], dq[yi(2)])
    osend[...] = down.astype(BF).reshape(XC, 32, Q)

    orecv[me] = osend[me]
    for i, g in enumerate(groups[1:], 1):
        send(osend.at[xc_to(g)], orecv.at[me], os_.at[i], or_.at[i], dev(dx=g[0], dc=g[1]))
    to_z, to_e = r_id // 16, r_id % 16
    source = (to_e // 2) * 32 + (to_e % 2) * 16 + to_z
    turn = jnp.where(l_id == source, 1.0, 0.0).astype(BF)
    for i, g in enumerate(groups[1:], 1):
        arrive(orecv.at[xc_from(g)], os_.at[i], or_.at[i])
    zsend[...] = dot(turn, orecv[...].reshape(256, Q)).astype(BF).reshape(NZ, 16, Q)
    zrecv[z] = zsend[z]
    for d in (8, 7, 9, 6, 10, 5, 11, 4, 12, 3, 13, 2, 14, 1, 15):
        send(zsend.at[zi(d)], zrecv.at[z], rets.at[d], retr.at[d], dev(dz=d))
    for d in range(1, NZ):
        arrive(zrecv.at[zi(-d)], rets.at[d], retr.at[d])
    back = zrecv[...].reshape(256, Q)
    both = dot(jnp.concatenate([comb_hi, comb_lo], axis=0), back)
    result = (after + (both[0:16] + both[16:32])).astype(BF)
    out_ref[...] = result[0:SEQ, :]
    store.wait()
    for copy in pending:
        copy.wait_send()


def shards(
    residual_in,
    rec_state,
    mix_gain,
    w_query,
    w_forget,
    w_input,
    w_gate,
    lower_bound,
    head_gain,
    w_out,
    ffn_gain,
    route_ids,
    route_weight,
    expert_gate,
    expert_up,
    expert_down,
):
    columns = jnp.concatenate(
        [w_query, w_forget, w_input, w_gate, w_out, jnp.zeros((Q, 4), BF)], axis=1
    ).T
    vmem = pl.BlockSpec(memory_space=pltpu.VMEM)
    hbm = pl.BlockSpec(memory_space=pl.ANY)
    dma = pltpu.SemaphoreType.DMA
    out = pl.pallas_call(
        kernel,
        out_shape=(
            jax.ShapeDtypeStruct((SEQ, Q), BF),
            jax.ShapeDtypeStruct(rec_state.shape, BF),
        ),
        in_specs=[vmem] * 8 + [hbm] * 4,
        out_specs=(vmem, hbm),
        scratch_shapes=[
            pltpu.VMEM((NZ, 64, Q), BF),
            pltpu.VMEM((XC, NZ, 16, Q), BF),
            pltpu.VMEM((XC, 16, Q), BF),
            pltpu.VMEM((NY, XC, 16, 256), BF),
            pltpu.VMEM((NY, XC, 16, 256), BF),
            pltpu.VMEM((1024, 1024), BF),
            pltpu.VMEM((SEQ, HL, HEAD, HEAD), BF),
            pltpu.VMEM((SEQ, HL, HEAD, HEAD), BF),
            pltpu.VMEM((2, HL, HEAD, 128), F32),
            pltpu.VMEM((HL, 16, HEAD), F32),
            pltpu.VMEM((HL, 16, HEAD), F32),
            pltpu.VMEM((16, Q), BF),
            pltpu.VMEM((NY, 16, 512), BF),
            pltpu.VMEM((NY, 16, 512), BF),
            pltpu.VMEM((16, 128), F32),
            pltpu.VMEM((NY, 16, 128), F32),
            pltpu.VMEM((16, D), F32),
            pltpu.VMEM((16, 128), jnp.int32),
            pltpu.VMEM((16, 128), F32),
            pltpu.VMEM((NZ, 16, Q), BF),
            pltpu.VMEM((XC, 32, Q), BF),
            pltpu.VMEM((NY, XC, 32, Q), BF),
            pltpu.VMEM((NY, 256, FQ), BF),
            pltpu.VMEM((NY, FQ, Q), BF),
            pltpu.VMEM((D, FQ), BF),
            pltpu.VMEM((D, FQ), BF),
            pltpu.VMEM((XC, 32, Q), BF),
            pltpu.VMEM((XC, 32, Q), BF),
            pltpu.VMEM((NZ, 16, Q), BF),
            pltpu.VMEM((NZ, 16, Q), BF),
        ]
        + [
            dma((n,))
            for n in (16, 16, 8, 8, 32, 32, 8, 8, 4, 4, 4, 4, 16, 16, 8, 8)
        ]
        + [dma((3, 8)), dma((3, 8))]
        + [dma((n,)) for n in (4, 4, 4, 4, 8, 8, 16, 16, 8)],
        compiler_params=pltpu.CompilerParams(
            collective_id=0, has_side_effects=True, vmem_limit_bytes=48 * 1024 * 1024
        ),
    )(
        residual_in,
        mix_gain.reshape(1, D),
        columns,
        lower_bound.reshape(1, Q),
        head_gain.reshape(1, HEAD),
        ffn_gain.reshape(1, D),
        route_ids,
        route_weight,
        rec_state,
        expert_gate.reshape(D, FQ),
        expert_up.reshape(D, FQ),
        expert_down.reshape(FQ, D),
    )
    return out


def solution(mesh):
    split = Mesh(mesh.devices.reshape(NZ, NX, NC, NY), ("ep_0", "ep_1", "ep_2", "tp"))
    in_specs = (
        P(EP, None),
        P(EP, "tp", None, None),
        P(),
        P("tp", EP),
        P("tp", EP),
        P("tp", EP),
        P("tp", EP),
        P("tp"),
        P(),
        P("tp", EP),
        P(),
        P(EP, None),
        P(EP, None),
        P(EP, None, "tp"),
        P(EP, None, "tp"),
        P(EP, "tp", None),
    )
    out_specs = (P(EP, "tp"), P(EP, "tp", None, None))
    return jax.shard_map(
        shards, mesh=split, in_specs=in_specs, out_specs=out_specs, check_vma=False
    )
```

time: 381 us -> 124 us (0.33)
  blocking collectives: 145 us -> 0 us
  waiting for transfers between devices: 108 us -> 0 us
  Pallas kernels: 0 us -> 107 us
  starting transfers between devices: 49.6 us -> 0 us
  local copies, waits for them, and re-layouts: 37.6 us -> 14.9 us
  other arithmetic: 15.6 us -> 0 us
  between operations: 14.5 us -> 0.65 us
  matrix products: 8.61 us -> 0 us
    pallas_call x0 -> x1, Pallas kernels: none -> 107 us  [shards(): pl.pallas_call(kernel, out_shape=(jax.ShapeDtypeStruct((SEQ, Q), BF), jax...]
    all_gather x6 -> x0, blocking collectives: 98.3 us -> none  [the longest x4 76.4 us: gather_in_order(): pieces = lax.all_gather(pieces, axes[k], axis=0, tiled=True)]
    all_to_all x5 -> x0, waiting for transfers between devices: 58.9 us -> none  [the longest x1 19.7 us: shards(): lax.all_to_all(partial_mix.astype(jnp.bfloat16), EP, split_axis=0, concat...]
    all_to_all x5 -> x0, starting transfers between devices: 49.5 us -> none  [the longest x1 15.2 us: shards(): lax.all_to_all(partial_mix.astype(jnp.bfloat16), EP, split_axis=0, concat...]
    all_gather x2 -> x0, waiting for transfers between devices: 49 us -> none  [gather_in_order(): pieces = lax.all_gather(pieces, axes[k], axis=0, tiled=True)]
    all_to_all x1 -> x0, blocking collectives: 33 us -> none  [shards(): lax.all_to_all(partial_proj.astype(jnp.bfloat16), EP, split_axis=0, conca...]
    transpose x5 -> x0, local copies, waits for them, and re-layouts: 18.1 us -> none  [the longest x4 15.9 us: split_up(): return jnp.moveaxis(pieces, dim, 0)]
    psum x1 -> x0, blocking collectives: 13.8 us -> none  [shards(): mixed = lax.psum(mixed_home.astype(jnp.bfloat16), 'tp').astype(jnp.float32)]
  transfers between devices with their start and end apart: 7 -> 0, of which waited for: 6 -> 0; matrix products, arithmetic and copies ran while one was open for 5% -> 0% of each run, Pallas kernels for 0% -> 0%
where the time goes in v1:
time: 124 us; the launch traced here: 122 us
  Pallas kernels  107 us (86%)
  local copies, waits for them, and re-layouts  14.9 us (12%)
    pallas_call x1, Pallas kernels, shards(): pl.pallas_call(kernel, out_shape=(jax.ShapeDtypeStruct((SEQ, Q), BF), jax...  107 us
    unnamed x16, local copies, waits for them, and re-layouts  9.07 us
    concatenate x1, local copies, waits for them, and re-layouts, shards(): jnp.concatenate([w_query, w_forget, w_input, w_gate, w_out, jnp.zeros((Q,...  3.77 us

profile of v1, /device:TPU:1, one launch (start us, length us, event | category | flops | bytes accessed | tf_op | source)
XLA Modules:
  0.0 122.2 jit_solution(5043063763846078494)
XLA Ops:
  0.6 0.7 reshape.26.lower_ref
  1.3 0.7 reshape.25.mix_gain_ref
  2.0 0.7 reshape.28.ffn_gain_ref
  2.7 0.8 copy.18.ids_ref
  3.5 0.8 copy.19.rw_ref
  4.3 3.8 %concatenate.3 = bf16[384,64]{0,1:T(8,128)(2,1)S(1)} concatenate(bf16[384,12]{0,1:T(8,128)(2,1)} %param.19, bf16[384,12]{0,1:T(8,128)(2,1)} %param.20, bf16[384,12]{0,1:T(8,128)(2,1)} %param.21, bf16[384,12]{0,1:T(8,128)(2,1)} %param.22, bf16[384,12]{0,1:T(8,128)(2,1)} %param.25, bf16[384,4]{0,1:T(4,128)(2,1)S(1)} %broadcast_in_dim.3), dimensions={1} | concatenate | bytes 98304 | tf_op jit(solution)/shard_map/concatenate | solution.py:509
  8.0 0.0 copy-start
  8.0 1.4 %copy-done = bf16[15,3,128,128]{3,2,1,0:T(8,128)(2,1)S(1)} copy-done((bf16[15,3,128,128]{3,2,1,0:T(8,128)(2,1)S(1)}, bf16[15,3,128,128]{3,2,1,0:T(8,128)(2,1)}, u32[]{:S(2)}) %copy-start) | copy-done | bytes 1474584
  9.4 0.0 copy-start.1
  9.4 1.0 copy-done.1
  10.4 0.0 copy-start.2
  10.4 1.0 copy-done.2
  11.4 0.0 copy-start.3
  11.4 1.0 copy-done.3
  12.4 0.0 copy-start.4
  12.4 0.8 copy-done.4
  13.2 0.0 copy-start.5
  13.2 0.7 copy-done.5
  13.9 106.6 %shard_map.167 = (bf16[15,384]{1,0:T(8,128)(2,1)S(1)}, bf16[15,3,128,128]{3,2,1,0:T(8,128)(2,1)S(1)}) custom-call(bf16[15,1536]{1,0:T(8,128)(2,1)S(1)} %copy-done.4, f32[1,1536]{1,0:T(1,128)S(1)} %reshape.25.mix_gain_ref, bf16[64,384]{1,0:T(8,128)(2,1)S(1)} %bitcast.8, f32[1,384]{1,0:T(1,128)S(1)} %reshape.26.lower_ref, f32[1,128]{1,0:T(1,128)S(1)} %bitcast.9, ...), custom_call_target="tpu_custom_call" | custom-call | tf_op jit(solution)/shard_map/pallas_call | solution.py:515
  120.5 0.6 copy.22
  121.1 1.1 copy.23
  (1 shorter events, 0.0 us)
Async XLA Ops:
  8.0 1.4 %copy-start = (bf16[15,3,128,128]{3,2,1,0:T(8,128)(2,1)S(1)}, bf16[15,3,128,128]{3,2,1,0:T(8,128)(2,1)}, u32[]{:S(2)}) copy-start(bf16[15,3,128,128]{3,2,1,0:T(8,128)(2,1)} %state_hbm.1) | copy-start | bytes 4423684
  9.4 1.0 copy-start.1
  10.4 1.0 copy-start.2
  11.4 1.0 copy-start.3
  12.4 0.8 copy-start.4
  13.2 0.7 copy-start.5

commit v2 on v1

--- a/solution.py
+++ b/solution.py
@@ -38,20 +38,33 @@
 
 
 def kernel(
-    res_ref,
-    mix_gain_ref,
-    w_ref,
-    lower_ref,
-    head_gain_ref,
-    ffn_gain_ref,
-    ids_ref,
-    rw_ref,
+    res_hbm,
+    wq_hbm,
+    wf_hbm,
+    wi_hbm,
+    wg_hbm,
+    wo_hbm,
+    mix_gain_hbm,
+    lower_hbm,
+    head_gain_hbm,
+    ffn_gain_hbm,
+    ids_hbm,
+    rw_hbm,
     state_hbm,
     eg_hbm,
     eu_hbm,
     ed_hbm,
     out_ref,
     new_state_hbm,
+    res_ref,
+    w_v,
+    w_all,
+    mix_gain_v,
+    lower_v,
+    head_gain_v,
+    ffn_gain_v,
+    ids_v,
+    rw_v,
     wz,
     wo,
     tok,
@@ -166,6 +179,26 @@
         pltpu.make_async_copy(eg_hbm, wg_v, local.at[1]),
         pltpu.make_async_copy(eu_hbm, wu_v, local.at[2]),
     ]
+    early = [
+        (wq_hbm, w_v.at[0]),
+        (wf_hbm, w_v.at[1]),
+        (wi_hbm, w_v.at[2]),
+        (wg_hbm, w_v.at[3]),
+        (wo_hbm, w_v.at[4]),
+        (res_hbm, res_ref),
+        (mix_gain_hbm, mix_gain_v),
+        (lower_hbm, lower_v),
+        (head_gain_hbm, head_gain_v),
+        (ffn_gain_hbm, ffn_gain_v),
+        (ids_hbm, ids_v),
+        (rw_hbm, rw_v),
+    ]
+    early = [
+        pltpu.make_async_copy(src, dst, local.at[8 + n])
+        for n, (src, dst) in enumerate(early)
+    ]
+    for copy in early:
+        copy.start()
 
     def quarter(ref, part):
         return ref.at[:, pl.ds(pl.multiple_of(part * Q, Q), Q)]
@@ -184,14 +217,21 @@
         )
 
     res_s[...] = jnp.zeros_like(res_s)
+    w_all[...] = jnp.zeros_like(w_all)
+    for copy in early:
+        copy.wait()
+    for n in range(5):
+        w_all[n * COLS : (n + 1) * COLS, :] = w_v[n].astype(F32)
+    wz[z] = w_all[...].astype(BF)
     res_s[0:SEQ, :] = res_ref[...].astype(F32)
-    own_w = pltpu.make_async_copy(w_ref, wz.at[z], local.at[4])
-    own_w.start()
     res = res_s[...]
+    mix_gain = mix_gain_v[pl.ds(pl.multiple_of(y * Q, Q), Q)].reshape(1, Q)
+    ffn_gain = ffn_gain_v[pl.ds(pl.multiple_of(y * Q, Q), Q)].reshape(1, Q)
+    lower_all = lower_v[...].reshape(1, Q)
+    head_gain = head_gain_v[...].reshape(1, HEAD)
     scale = lax.rsqrt(jnp.mean(res * res, axis=-1, keepdims=True) + EPS)
     own = pl.ds(pl.multiple_of(y * Q, Q), Q)
-    tok[me] = (res_s[:, own] * scale * mix_gain_ref[:, own]).astype(BF)
-    own_w.wait()
+    tok[me] = (res_s[:, own] * scale * mix_gain).astype(BF)
     pl.semaphore_wait(barrier, len(peers))
 
     def z_start(buf, ss, rs):
@@ -234,13 +274,13 @@
     for k in range(1, NY):
         send(quarter(ed_hbm, yi(k)), dq.at[y], ds_.at[k], dr.at[k], dev(dy=k))
 
-    ids_s[...] = jnp.full_like(ids_s, -1)
-    ids_s[0:SEQ, 0:TOPK] = ids_ref[...]
+    ids_s[...] = jnp.full_like(ids_s, -1.0)
+    ids_s[0:TOPK, 0:SEQ] = ids_v[...].astype(F32)
     rw_s[...] = jnp.zeros_like(rw_s)
-    rw_s[0:SEQ, 0:TOPK] = rw_ref[...]
-    ids, rw = ids_s[...], rw_s[...]
+    rw_s[0:TOPK, 0:SEQ] = rw_v[...]
+    ids, rw = jnp.transpose(ids_s[...])[0:16], jnp.transpose(rw_s[...])[0:16]
     lane = iota((16, 256), 1)
-    expert, slot = lane // 2, lane % 2
+    expert, slot = (lane // 2).astype(F32), lane % 2
     row = iota((16, 256), 0).astype(F32)
     named = jnp.zeros((16, 256), F32)
     weight = jnp.zeros((16, 256), F32)
@@ -319,7 +359,7 @@
         )
     gates = []
     for h in range(HL):
-        lower = lower_ref[:, h * HEAD : (h + 1) * HEAD]
+        lower = lower_all[:, h * HEAD : (h + 1) * HEAD]
         query = proj[0][h] * sigmoid(proj[0][h])
         forget = lower + (1.0 - lower) * sigmoid(proj[1][h])
         for n, values in enumerate((query, forget)):
@@ -348,7 +388,7 @@
     for h in range(HL):
         r = read_s[h]
         r = r * lax.rsqrt(jnp.mean(r * r, axis=-1, keepdims=True) + EPS)
-        ho[:, h * HEAD : (h + 1) * HEAD] = (r * head_gain_ref[...] * gates[h]).astype(BF)
+        ho[:, h * HEAD : (h + 1) * HEAD] = (r * head_gain * gates[h]).astype(BF)
 
     for dx in range(1, NX):
         src = lax.rem(x - dx + NX, NX) * NC + c
@@ -384,7 +424,7 @@
     srecv[y] = ssend[...]
     for k in range(1, NY):
         send(ssend, srecv.at[y], sss.at[k], ssr.at[k], dev(dy=k))
-    gained = after * ffn_gain_ref[:, own]
+    gained = after * ffn_gain
     table_row = jnp.concatenate([table, jnp.zeros((1, 128), F32)], axis=1)
     is_table = iota((16, Q), 0) == SEQ
     for k in range(1, NY):
@@ -506,9 +546,6 @@
     expert_up,
     expert_down,
 ):
-    columns = jnp.concatenate(
-        [w_query, w_forget, w_input, w_gate, w_out, jnp.zeros((Q, 4), BF)], axis=1
-    ).T
     vmem = pl.BlockSpec(memory_space=pltpu.VMEM)
     hbm = pl.BlockSpec(memory_space=pl.ANY)
     dma = pltpu.SemaphoreType.DMA
@@ -518,9 +555,18 @@
             jax.ShapeDtypeStruct((SEQ, Q), BF),
             jax.ShapeDtypeStruct(rec_state.shape, BF),
         ),
-        in_specs=[vmem] * 8 + [hbm] * 4,
+        in_specs=[hbm] * 16,
         out_specs=(vmem, hbm),
         scratch_shapes=[
+            pltpu.VMEM((SEQ, D), BF),
+            pltpu.VMEM((5, COLS, Q), BF),
+            pltpu.VMEM((64, Q), F32),
+            pltpu.VMEM((D,), F32),
+            pltpu.VMEM((Q,), F32),
+            pltpu.VMEM((HEAD,), F32),
+            pltpu.VMEM((D,), F32),
+            pltpu.VMEM((TOPK, SEQ), jnp.int32),
+            pltpu.VMEM((TOPK, SEQ), F32),
             pltpu.VMEM((NZ, 64, Q), BF),
             pltpu.VMEM((XC, NZ, 16, Q), BF),
             pltpu.VMEM((XC, 16, Q), BF),
@@ -538,8 +584,8 @@
             pltpu.VMEM((16, 128), F32),
             pltpu.VMEM((NY, 16, 128), F32),
             pltpu.VMEM((16, D), F32),
-            pltpu.VMEM((16, 128), jnp.int32),
-            pltpu.VMEM((16, 128), F32),
+            pltpu.VMEM((128, 128), F32),
+            pltpu.VMEM((128, 128), F32),
             pltpu.VMEM((NZ, 16, Q), BF),
             pltpu.VMEM((XC, 32, Q), BF),
             pltpu.VMEM((NY, XC, 32, Q), BF),
@@ -557,19 +603,23 @@
             for n in (16, 16, 8, 8, 32, 32, 8, 8, 4, 4, 4, 4, 16, 16, 8, 8)
         ]
         + [dma((3, 8)), dma((3, 8))]
-        + [dma((n,)) for n in (4, 4, 4, 4, 8, 8, 16, 16, 8)],
+        + [dma((n,)) for n in (4, 4, 4, 4, 8, 8, 16, 16, 20)],
         compiler_params=pltpu.CompilerParams(
-            collective_id=0, has_side_effects=True, vmem_limit_bytes=48 * 1024 * 1024
+            collective_id=0, has_side_effects=True, vmem_limit_bytes=63 * 1024 * 1024
         ),
     )(
         residual_in,
-        mix_gain.reshape(1, D),
-        columns,
-        lower_bound.reshape(1, Q),
-        head_gain.reshape(1, HEAD),
-        ffn_gain.reshape(1, D),
-        route_ids,
-        route_weight,
+        w_query.T,
+        w_forget.T,
+        w_input.T,
+        w_gate.T,
+        w_out.T,
+        mix_gain,
+        lower_bound,
+        head_gain,
+        ffn_gain,
+        route_ids.T,
+        route_weight.T,
         rec_state,
         expert_gate.reshape(D, FQ),
         expert_up.reshape(D, FQ),

time: 124 us -> 113 us (0.911)
  local copies, waits for them, and re-layouts: 14.9 us -> 3.96 us
    unnamed x16 -> x2, local copies, waits for them, and re-layouts: 9.07 us -> 3.96 us
    concatenate x1 -> x0, local copies, waits for them, and re-layouts: 3.77 us -> none  [shards(): jnp.concatenate([w_query, w_forget, w_input, w_gate, w_out, jnp.zeros((Q,...]
    reshape x3 -> x0, local copies, waits for them, and re-layouts: 2.09 us -> none  [the longest x1 0.7 us: shards(): mix_gain.reshape(1, D)]
where the time goes in v2:
time: 113 us; the launch traced here: 112 us
  Pallas kernels  107 us (95%)
  local copies, waits for them, and re-layouts  3.96 us (4%)
    pallas_call x1, Pallas kernels, shards(): pl.pallas_call(kernel, out_shape=(jax.ShapeDtypeStruct((SEQ, Q), BF), jax...  107 us
    unnamed x2, local copies, waits for them, and re-layouts  3.96 us

profile of v2, /device:TPU:1, one launch (start us, length us, event | category | flops | bytes accessed | tf_op | source)
XLA Modules:
  0.0 111.7 jit_solution(5780468947717320760)
XLA Ops:
  0.6 107.1 %shard_map.167 = (bf16[15,384]{1,0:T(8,128)(2,1)}, bf16[15,3,128,128]{3,2,1,0:T(8,128)(2,1)}) custom-call(bf16[15,1536]{1,0:T(8,128)(2,1)} %res_hbm.1, bf16[12,384]{1,0:T(8,128)(2,1)} %bitcast.13, bf16[12,384]{1,0:T(8,128)(2,1)} %bitcast.14, bf16[12,384]{1,0:T(8,128)(2,1)} %bitcast.15, bf16[12,384]{1,0:T(8,128)(2,1)} %bitcast.16, bf16[12,384]{1,0:T(8,128)(2,1)} %bitcast.17, ...), custom_call_target="tpu_custom_call" | custom-call | tf_op jit(solution)/shard_map/pallas_call | solution.py:552
  107.8 1.3 %copy.20 = bf16[15,384]{1,0:T(8,128)(2,1)} copy(bf16[15,384]{1,0:T(8,128)(2,1)} %get-tuple-element.4) | data formatting | bytes 23040
  109.1 2.7 %copy.21 = bf16[15,3,128,128]{3,2,1,0:T(8,128)(2,1)} copy(bf16[15,3,128,128]{3,2,1,0:T(8,128)(2,1)} %get-tuple-element.5) | data formatting | bytes 2949120

commit v3 on v2

--- a/solution.py
+++ b/solution.py
@@ -68,6 +68,8 @@
     wz,
     wo,
     tok,
+    hall,
+    order_out,
     psend,
     precv,
     perm_in,
@@ -101,8 +103,10 @@
     tokr,
     ps,
     pr,
-    wos,
-    wor,
+    hgs,
+    hgr,
+    z3s,
+    z3r,
     rss,
     rsr,
     sss,
@@ -206,7 +210,7 @@
     own_down = pltpu.make_async_copy(quarter(ed_hbm, y), dq.at[y], local.at[3])
 
     barrier = pltpu.get_barrier_semaphore()
-    peers = [dict(dz=d) for d in range(1, NZ)]
+    peers = [dict(dz=d) for d in (1, -1, 4, -4)]
     for g in groups:
         for dy in range(NY):
             if g != (0, 0) or dy:
@@ -222,7 +226,8 @@
         copy.wait()
     for n in range(5):
         w_all[n * COLS : (n + 1) * COLS, :] = w_v[n].astype(F32)
-    wz[z] = w_all[...].astype(BF)
+    wz[:, 48:64, :] = jnp.zeros((NZ, 16, Q), BF)
+    wz[z, 0:48, :] = w_all[0:48, :].astype(BF)
     res_s[0:SEQ, :] = res_ref[...].astype(F32)
     res = res_s[...]
     mix_gain = mix_gain_v[pl.ds(pl.multiple_of(y * Q, Q), Q)].reshape(1, Q)
@@ -234,38 +239,90 @@
     tok[me] = (res_s[:, own] * scale * mix_gain).astype(BF)
     pl.semaphore_wait(barrier, len(peers))
 
-    def z_start(buf, ss, rs):
-        for k, d in ((2, 4), (3, -4), (0, 1), (1, -1), (4, 2), (5, -2)):
-            send(buf.at[z], buf.at[z], ss.at[k], rs.at[k], dev(dz=d))
-
-    def z_finish(buf, ss, rs, first, second):
-        def block(d, part=None):
-            ref = buf.at[zi(d)]
-            return ref if part is None else ref.at[part]
-
-        def pass_on(k, d, to, part=None):
-            send(block(d, part), block(d, part), ss.at[k], rs.at[k], dev(dz=to))
-
-        def got(k, d, part=None):
-            arrive(block(d, part), ss.at[k], rs.at[k])
-
+    def z_ways(view, ss, rs):
+        def pass_on(k, d, to, half=None):
+            send(view(d, half), view(d, half), ss.at[k], rs.at[k], dev(dz=to))
+
+        def got(k, d, half=None):
+            arrive(view(d, half), ss.at[k], rs.at[k])
+
+        return pass_on, got
+
+    def lean_start(ways):
+        pass_on, _ = ways
+        for k, to in ((2, 4), (3, -4), (0, 1), (1, -1)):
+            pass_on(k, 0, to)
+
+    def lean_middle(ways):
+        pass_on, got = ways
+        got(0, -1)
+        pass_on(4, -1, 1)
+        got(1, 1)
+        pass_on(5, 1, -1)
         got(2, -4)
-        pass_on(6, -4, 4, first)
+        pass_on(6, -4, 4, 0)
         got(3, 4)
-        pass_on(10, 4, -4, second)
-        for k, d, to in ((7, -4, 1), (8, -4, -1), (9, -4, 2), (11, 4, 1), (12, 4, -1), (13, 4, -2)):
+        pass_on(10, 4, -4, 1)
+        for k, d, to in ((7, -4, 1), (12, 4, -1), (8, -4, -1), (11, 4, 1)):
             pass_on(k, d, to)
-        got(6, 8, first)
-        got(10, 8, second)
+        got(7, -5)
+        pass_on(9, -5, 1)
+        got(12, 5)
+        pass_on(13, 5, -1)
+
+    def lean_last(ways):
+        pass_on, got = ways
+        got(6, 8, 0)
+        got(10, 8, 1)
         pass_on(14, 8, 1)
         pass_on(15, 8, -1)
-        for k, d in (
-            (0, -1), (1, 1), (4, -2), (5, 2), (7, -5), (8, -3),
-            (9, -6), (11, 3), (12, 5), (13, 6), (14, 7), (15, 9),
-        ):
+
+    def lean_rest(ways):
+        _, got = ways
+        for k, d in ((4, -2), (5, 2), (8, -3), (9, -6), (11, 3), (13, 6), (14, 7), (15, 9)):
             got(k, d)
 
-    z_start(wz, z1s, z1r)
+    def quick_start(ways):
+        pass_on, _ = ways
+        for k, to in ((6, 6), (7, -6), (4, 4), (5, -4), (2, 2), (3, -2), (0, 1), (1, -1)):
+            pass_on(k, 0, to)
+
+    def quick_finish(ways):
+        pass_on, got = ways
+        got(4, -4)
+        pass_on(8, -4, -1)
+        got(5, 4)
+        pass_on(9, 4, 1)
+        got(6, -6)
+        pass_on(10, -6, 2, 0)
+        pass_on(12, -6, 1)
+        pass_on(13, -6, -1)
+        got(7, 6)
+        pass_on(11, 6, -2, 1)
+        pass_on(14, 6, -1)
+        pass_on(15, 6, 1)
+        for k, d in ((0, -1), (1, 1), (2, -2), (3, 2), (8, -3), (9, 3), (12, -7), (13, -5), (14, 7), (15, 5)):
+            got(k, d)
+        got(10, 8, 0)
+        got(11, 8, 1)
+
+    def lanes_of(buf):
+        def view(d, half):
+            ref = buf.at[zi(d)]
+            if half is None:
+                return ref
+            return ref.at[:, pl.ds(0, 256)] if half == 0 else ref.at[:, pl.ds(256, 128)]
+
+        return view
+
+    def rows_of(d, half):
+        first, count = ((0, 48), (0, 32), (32, 16))[0 if half is None else half + 1]
+        return wz.at[zi(d), pl.ds(first, count)]
+
+    in_ways = z_ways(rows_of, z1s, z1r)
+    out_ways = z_ways(lanes_of(wo), z3s, z3r)
+    tok_ways = z_ways(lanes_of(tz), z2s, z2r)
+    lean_start(in_ways)
     for i, g in enumerate(groups[1:], 1):
         send(tok.at[me], tok.at[me], toks.at[i], tokr.at[i], dev(dx=g[0], dc=g[1]))
     for copy in loads:
@@ -295,6 +352,10 @@
     combine = jnp.where(row == table, weight, 0.0)
     comb_hi, comb_lo = split_two(combine)
 
+    table_row = jnp.concatenate([table, jnp.zeros((1, 128), F32)], axis=1)
+    wo[z] = jnp.where(iota((16, Q), 0) == COLS, table_row, w_all[48:64, :]).astype(BF)
+    lean_start(out_ways)
+
     k_id = iota((1024, 1), 0)
     k_xc, k_in = k_id // 128, k_id % 128
     k_q, k_pj = k_in // 64, k_in % 64
@@ -302,12 +363,17 @@
     target = jnp.where(k_pj < 48, k_p * 256 + k_q * 96 + COLS * k_xc + k_j, -1)
     order_in = jnp.where(iota((1024, 1024), 1) == target, 1.0, 0.0).astype(BF)
     perm_in[...] = order_in
-
-    z_finish(wz, z1s, z1r, (pl.ds(0, 32),), (pl.ds(32, 32),))
-
-    wo_own = wz.at[:, pl.ds(48, 16), :]
-    own_wo = pltpu.make_async_copy(wo_own, wo.at[me], local.at[5])
-    own_wo.start()
+    o_id = iota((1024, 1), 0)
+    o_xc, o_half, o_q, o_j = o_id // 128, (o_id // 64) % 2, (o_id // 16) % 4, o_id % 16
+    o_ok = (o_j < COLS) & (o_half == lax.rem(y, 2))
+    o_to = jnp.where(o_ok, 96 * o_q + COLS * o_xc + o_j, -1)
+    order_out[...] = jnp.where(iota((1024, Q), 1) == o_to, 1.0, 0.0).astype(BF)
+
+    lean_middle(in_ways)
+    lean_middle(out_ways)
+    lean_last(in_ways)
+    lean_rest(in_ways)
+
     for i, g in enumerate(groups[1:], 1):
         arrive(tok.at[xc_from(g)], toks.at[i], tokr.at[i])
     tokens = tok[...].reshape(XC * 16, Q)
@@ -328,9 +394,7 @@
             pr.at[i],
             dev(dx=g[0], dc=g[1], dy=dy),
         )
-    for dx in range(1, NX):
-        send(wo_own, wo.at[me], wos.at[dx], wor.at[dx], dev(dx=dx))
-    send(wo_own, wo.at[me], wos.at[0], wor.at[0], dev(dc=1))
+    lean_last(out_ways)
 
     for i, (g, dy) in enumerate(pairs):
         if i:
@@ -390,34 +454,36 @@
         r = r * lax.rsqrt(jnp.mean(r * r, axis=-1, keepdims=True) + EPS)
         ho[:, h * HEAD : (h + 1) * HEAD] = (r * head_gain * gates[h]).astype(BF)
 
-    for dx in range(1, NX):
-        src = lax.rem(x - dx + NX, NX) * NC + c
-        arrive(wo.at[src], wos.at[dx], wor.at[dx])
-        send(wo.at[src], wo.at[src], wos.at[NX + dx], wor.at[NX + dx], dev(dc=1))
-    other = 1 - c
-    arrive(wo.at[x * NC + other], wos.at[0], wor.at[0])
-    for dx in range(1, NX):
-        src = lax.rem(x - dx + NX, NX) * NC + other
-        arrive(wo.at[src], wos.at[NX + dx], wor.at[NX + dx])
-    own_wo.wait()
-    heads = ho[...]
-    for k in (1, 2, 3, 0):
-        part = yi(k)
-        block = wo[:, pl.ds(4 * part, 4)].reshape(512, Q)
-        rsend[part] = dot_t(heads, block).astype(BF)
-        if k:
-            send(rsend.at[part], rrecv.at[y], rss.at[k], rsr.at[k], dev(dy=k))
-    rrecv[y] = rsend[y]
-    o_id = iota((512, 1), 0)
-    o_xc, o_q, o_j = o_id // 64, (o_id // 16) % 4, o_id % 16
-    o_to = jnp.where(o_j < COLS, 96 * o_q + COLS * o_xc + o_j, -1)
-    order_out = jnp.where(iota((512, Q), 1) == o_to, 1.0, 0.0).astype(BF)
-    for k in range(1, NY):
-        arrive(rrecv.at[yi(-k)], rss.at[k], rsr.at[k])
-    total = rrecv[0].astype(F32)
-    for k in range(1, NY):
-        total = total + rrecv[k].astype(F32)
-    both = dot(jnp.concatenate(split_two(total), axis=0), order_out)
+    hall[me] = ho[...]
+    for i, g in enumerate(groups[1:], 1):
+        send(hall.at[me], hall.at[me], hgs.at[i], hgr.at[i], dev(dx=g[0], dc=g[1]))
+    lean_rest(out_ways)
+    for i, g in enumerate(groups[1:], 1):
+        arrive(hall.at[xc_from(g)], hgs.at[i], hgr.at[i])
+    mixed = dot_t(hall[...].reshape(128, Q), wo[...].reshape(256, Q)).astype(BF)
+    for h in range(2):
+        rsend[h] = mixed[:, 128 * h : 128 * h + 128].reshape(XC, 16, 128)
+    rrecv[y, me] = rsend[y // 2, me]
+    for i, (g, dy) in enumerate(pairs):
+        if i:
+            send(
+                rsend.at[yi(dy) // 2, xc_to(g)],
+                rrecv.at[y, me],
+                rss.at[i],
+                rsr.at[i],
+                dev(dx=g[0], dc=g[1], dy=dy),
+            )
+    for i, (g, dy) in enumerate(pairs):
+        if i:
+            arrive(rrecv.at[yi(-dy), xc_from(g)], rss.at[i], rsr.at[i])
+    sums = []
+    for e in range(XC):
+        total = rrecv[0, e].astype(F32)
+        for k in range(1, NY):
+            total = total + rrecv[k, e].astype(F32)
+        sums.append(total)
+    total = jnp.concatenate(sums, axis=1)
+    both = dot(jnp.concatenate(split_two(total), axis=0), order_out[...])
     after = (res_s[:, own] + (both[0:16] + both[16:32])).astype(BF).astype(F32)
     square = jnp.sum(after * after, axis=-1, keepdims=True)
     ssend[...] = jnp.broadcast_to(square, (16, 128))
@@ -425,29 +491,27 @@
     for k in range(1, NY):
         send(ssend, srecv.at[y], sss.at[k], ssr.at[k], dev(dy=k))
     gained = after * ffn_gain
-    table_row = jnp.concatenate([table, jnp.zeros((1, 128), F32)], axis=1)
-    is_table = iota((16, Q), 0) == SEQ
     for k in range(1, NY):
         arrive(srecv.at[yi(-k)], sss.at[k], ssr.at[k])
     square = srecv[0] + srecv[1] + srecv[2] + srecv[3]
     inverse = lax.rsqrt(square[:, 0:1] * (1.0 / D) + EPS)
-    tz[z] = jnp.where(is_table, table_row, gained * inverse).astype(BF)
-
-    z_start(tz, z2s, z2r)
+    tz[z] = (gained * inverse).astype(BF)
+
+    quick_start(tok_ways)
     r_id, l_id = iota((256, 256), 0), iota((256, 256), 1)
-    spread = jnp.where((r_id // 16 == l_id // 16) & (l_id % 16 == SEQ), 1.0, 0.0).astype(BF)
+    spread = jnp.where((r_id // 16 == l_id // 16) & (l_id % 16 == COLS), 1.0, 0.0).astype(BF)
     mine = jnp.where(iota((16, 256), 1) == 16 * z + iota((16, 256), 0), 1.0, 0.0).astype(BF)
     same = iota((16, 256), 0) == iota((16, 256), 1) // 16
     token = (iota((16, 256), 1) % 16).astype(F32)
     loads[1].wait()
     loads[2].wait()
-    z_finish(tz, z2s, z2r, (slice(None), pl.ds(0, 256)), (slice(None), pl.ds(256, 128)))
-    flat = tz[...].reshape(256, Q)
-    tables = dot(spread, flat[:, 0:256]).astype(BF)
+    tables = dot(spread, wo[...].reshape(256, Q)[:, 0:256]).astype(BF)
     wanted = dot_t(mine, tables)
     hit = jnp.where(wanted == token, 1.0, 0.0)
     same_f = jnp.where(same, 1.0, 0.0)
     pick = (hit[:, None, :] * same_f[None, :, :]).reshape(256, 256).astype(BF)
+    quick_finish(tok_ways)
+    flat = tz[...].reshape(256, Q)
     xsend[...] = dot(pick, flat).astype(BF).reshape(XC, 32, Q)
     xf[y, me] = xsend[me]
     for i, g in enumerate(groups[1:], 1):
@@ -547,7 +611,8 @@
     expert_down,
 ):
     vmem = pl.BlockSpec(memory_space=pltpu.VMEM)
-    hbm = pl.BlockSpec(memory_space=pl.ANY)
+    hbm = pl.BlockSpec(memory_space=pltpu.HBM)
+    anywhere = pl.BlockSpec(memory_space=pl.ANY)
     dma = pltpu.SemaphoreType.DMA
     out = pl.pallas_call(
         kernel,
@@ -556,7 +621,7 @@
             jax.ShapeDtypeStruct(rec_state.shape, BF),
         ),
         in_specs=[hbm] * 16,
-        out_specs=(vmem, hbm),
+        out_specs=(vmem, anywhere),
         scratch_shapes=[
             pltpu.VMEM((SEQ, D), BF),
             pltpu.VMEM((5, COLS, Q), BF),
@@ -568,8 +633,10 @@
             pltpu.VMEM((TOPK, SEQ), jnp.int32),
             pltpu.VMEM((TOPK, SEQ), F32),
             pltpu.VMEM((NZ, 64, Q), BF),
-            pltpu.VMEM((XC, NZ, 16, Q), BF),
+            pltpu.VMEM((NZ, 16, Q), BF),
             pltpu.VMEM((XC, 16, Q), BF),
+            pltpu.VMEM((XC, 16, Q), BF),
+            pltpu.VMEM((1024, Q), BF),
             pltpu.VMEM((NY, XC, 16, 256), BF),
             pltpu.VMEM((NY, XC, 16, 256), BF),
             pltpu.VMEM((1024, 1024), BF),
@@ -579,8 +646,8 @@
             pltpu.VMEM((HL, 16, HEAD), F32),
             pltpu.VMEM((HL, 16, HEAD), F32),
             pltpu.VMEM((16, Q), BF),
-            pltpu.VMEM((NY, 16, 512), BF),
-            pltpu.VMEM((NY, 16, 512), BF),
+            pltpu.VMEM((2, XC, 16, 128), BF),
+            pltpu.VMEM((NY, XC, 16, 128), BF),
             pltpu.VMEM((16, 128), F32),
             pltpu.VMEM((NY, 16, 128), F32),
             pltpu.VMEM((16, D), F32),
@@ -600,7 +667,7 @@
         ]
         + [
             dma((n,))
-            for n in (16, 16, 8, 8, 32, 32, 8, 8, 4, 4, 4, 4, 16, 16, 8, 8)
+            for n in (16, 16, 8, 8, 32, 32, 8, 8, 16, 16, 32, 32, 4, 4, 16, 16, 8, 8)
         ]
         + [dma((3, 8)), dma((3, 8))]
         + [dma((n,)) for n in (4, 4, 4, 4, 8, 8, 16, 16, 20)],

time: 113 us -> 112 us (level); the launches traced: 112 us -> 112 us
  no operation moved by 1% of the time
where the time goes in v3:
time: 112 us
  Pallas kernels  107 us (96%)
  local copies, waits for them, and re-layouts  3.96 us (4%)
    pallas_call x1, Pallas kernels, shards(): pl.pallas_call(kernel, out_shape=(jax.ShapeDtypeStruct((SEQ, Q), BF), jax...  107 us
    unnamed x2, local copies, waits for them, and re-layouts  3.96 us

profile of v3, /device:TPU:1, one launch (start us, length us, event | category | flops | bytes accessed | tf_op | source)
XLA Modules:
  0.0 112.0 jit_solution(7976660555564084560)
XLA Ops:
  0.6 107.4 %shard_map.167 = (bf16[15,384]{1,0:T(8,128)(2,1)}, bf16[15,3,128,128]{3,2,1,0:T(8,128)(2,1)}) custom-call(bf16[15,1536]{1,0:T(8,128)(2,1)} %res_hbm.1, bf16[12,384]{1,0:T(8,128)(2,1)} %bitcast.13, bf16[12,384]{1,0:T(8,128)(2,1)} %bitcast.14, bf16[12,384]{1,0:T(8,128)(2,1)} %bitcast.15, bf16[12,384]{1,0:T(8,128)(2,1)} %bitcast.16, bf16[12,384]{1,0:T(8,128)(2,1)} %bitcast.17, ...), custom_call_target="tpu_custom_call" | custom-call | tf_op jit(solution)/shard_map/pallas_call | solution.py:617
  108.0 1.3 %copy.20 = bf16[15,384]{1,0:T(8,128)(2,1)} copy(bf16[15,384]{1,0:T(8,128)(2,1)} %get-tuple-element.4) | data formatting | bytes 23040
  109.3 2.7 %copy.21 = bf16[15,3,128,128]{3,2,1,0:T(8,128)(2,1)} copy(bf16[15,3,128,128]{3,2,1,0:T(8,128)(2,1)} %get-tuple-element.5) | data formatting | bytes 2949120

commit v4 on v3

--- a/solution.py
+++ b/solution.py
@@ -287,7 +287,7 @@
         for k, to in ((6, 6), (7, -6), (4, 4), (5, -4), (2, 2), (3, -2), (0, 1), (1, -1)):
             pass_on(k, 0, to)
 
-    def quick_finish(ways):
+    def quick_middle(ways):
         pass_on, got = ways
         got(4, -4)
         pass_on(8, -4, -1)
@@ -301,6 +301,9 @@
         pass_on(11, 6, -2, 1)
         pass_on(14, 6, -1)
         pass_on(15, 6, 1)
+
+    def quick_rest(ways):
+        _, got = ways
         for k, d in ((0, -1), (1, 1), (2, -2), (3, 2), (8, -3), (9, 3), (12, -7), (13, -5), (14, 7), (15, 5)):
             got(k, d)
         got(10, 8, 0)
@@ -354,7 +357,6 @@
 
     table_row = jnp.concatenate([table, jnp.zeros((1, 128), F32)], axis=1)
     wo[z] = jnp.where(iota((16, Q), 0) == COLS, table_row, w_all[48:64, :]).astype(BF)
-    lean_start(out_ways)
 
     k_id = iota((1024, 1), 0)
     k_xc, k_in = k_id // 128, k_id % 128
@@ -370,8 +372,8 @@
     order_out[...] = jnp.where(iota((1024, Q), 1) == o_to, 1.0, 0.0).astype(BF)
 
     lean_middle(in_ways)
-    lean_middle(out_ways)
     lean_last(in_ways)
+    quick_start(out_ways)
     lean_rest(in_ways)
 
     for i, g in enumerate(groups[1:], 1):
@@ -394,11 +396,10 @@
             pr.at[i],
             dev(dx=g[0], dc=g[1], dy=dy),
         )
-    lean_last(out_ways)
-
     for i, (g, dy) in enumerate(pairs):
         if i:
             arrive(precv.at[yi(-dy), xc_from(g)], ps.at[i], pr.at[i])
+    quick_middle(out_ways)
     halves = [[], []]
     for e in range(XC):
         total = precv[0, e].astype(F32)
@@ -457,7 +458,7 @@
     hall[me] = ho[...]
     for i, g in enumerate(groups[1:], 1):
         send(hall.at[me], hall.at[me], hgs.at[i], hgr.at[i], dev(dx=g[0], dc=g[1]))
-    lean_rest(out_ways)
+    quick_rest(out_ways)
     for i, g in enumerate(groups[1:], 1):
         arrive(hall.at[xc_from(g)], hgs.at[i], hgr.at[i])
     mixed = dot_t(hall[...].reshape(128, Q), wo[...].reshape(256, Q)).astype(BF)
@@ -510,7 +511,8 @@
     hit = jnp.where(wanted == token, 1.0, 0.0)
     same_f = jnp.where(same, 1.0, 0.0)
     pick = (hit[:, None, :] * same_f[None, :, :]).reshape(256, 256).astype(BF)
-    quick_finish(tok_ways)
+    quick_middle(tok_ways)
+    quick_rest(tok_ways)
     flat = tz[...].reshape(256, Q)
     xsend[...] = dot(pick, flat).astype(BF).reshape(XC, 32, Q)
     xf[y, me] = xsend[me]
@@ -617,8 +619,8 @@
     out = pl.pallas_call(
         kernel,
         out_shape=(
-            jax.ShapeDtypeStruct((SEQ, Q), BF),
-            jax.ShapeDtypeStruct(rec_state.shape, BF),
+            pltpu.VMEM((SEQ, Q), BF),
+            pltpu.VMEM(rec_state.shape, BF),
         ),
         in_specs=[hbm] * 16,
         out_specs=(vmem, anywhere),
@@ -672,7 +674,7 @@
         + [dma((3, 8)), dma((3, 8))]
         + [dma((n,)) for n in (4, 4, 4, 4, 8, 8, 16, 16, 20)],
         compiler_params=pltpu.CompilerParams(
-            collective_id=0, has_side_effects=True, vmem_limit_bytes=63 * 1024 * 1024
+            collective_id=0, has_side_effects=True, vmem_limit_bytes=60 * 1024 * 1024
         ),
     )(
         residual_in,

time: 112 us -> 106 us (0.946)
  the two profiles are of different devices: /device:TPU:1 before, /device:TPU:8 now
where the time goes in v4:
time: 106 us
  Pallas kernels  104 us (98%)
  local copies, waits for them, and re-layouts  1.71 us (2%)
    pallas_call x1, Pallas kernels, shards(): pl.pallas_call(kernel, out_shape=(pltpu.VMEM((SEQ, Q), BF), pltpu.VMEM(re...  104 us

profile of v4, /device:TPU:8, one launch (start us, length us, event | category | flops | bytes accessed | tf_op | source)
XLA Modules:
  0.0 106.2 jit_solution(9098679234474062275)
XLA Ops:
  0.6 103.8 %shard_map.167 = (bf16[15,384]{1,0:T(8,128)(2,1)S(1)}, bf16[15,3,128,128]{3,2,1,0:T(8,128)(2,1)S(1)}) custom-call(bf16[15,1536]{1,0:T(8,128)(2,1)} %res_hbm.1, bf16[12,384]{1,0:T(8,128)(2,1)} %bitcast.13, bf16[12,384]{1,0:T(8,128)(2,1)} %bitcast.14, bf16[12,384]{1,0:T(8,128)(2,1)} %bitcast.15, bf16[12,384]{1,0:T(8,128)(2,1)} %bitcast.16, ...), custom_call_target="tpu_custom_call" | custom-call | tf_op jit(solution)/shard_map/pallas_call | solution.py:619
  104.5 0.6 copy.20
  105.1 1.1 %copy.21 = bf16[15,3,128,128]{3,2,1,0:T(8,128)(2,1)} copy(bf16[15,3,128,128]{3,2,1,0:T(8,128)(2,1)S(1)} %get-tuple-element.3) | data formatting | bytes 2949120

commit v5 on v4

--- a/solution.py
+++ b/solution.py
@@ -81,8 +81,8 @@
     ho,
     rsend,
     rrecv,
-    ssend,
-    srecv,
+    res_p,
+    sum_s,
     res_s,
     ids_s,
     rw_s,
@@ -109,8 +109,6 @@
     z3r,
     rss,
     rsr,
-    sss,
-    ssr,
     z2s,
     z2r,
     xs,
@@ -370,6 +368,13 @@
     o_ok = (o_j < COLS) & (o_half == lax.rem(y, 2))
     o_to = jnp.where(o_ok, 96 * o_q + COLS * o_xc + o_j, -1)
     order_out[...] = jnp.where(iota((1024, Q), 1) == o_to, 1.0, 0.0).astype(BF)
+
+    home = res_s[...].astype(BF)
+    f_id, l_one = iota((D, 1), 0), iota((D, 256), 1)
+    for e in range(XC):
+        f_in = f_id % 96 - COLS * e
+        f_to = jnp.where((f_in >= 0) & (f_in < COLS), 16 * (f_id // 96) + f_in, -1)
+        res_p[e] = dot(home, jnp.where(l_one == f_to, 1.0, 0.0).astype(BF))
 
     lean_middle(in_ways)
     lean_last(in_ways)
@@ -462,13 +467,12 @@
     for i, g in enumerate(groups[1:], 1):
         arrive(hall.at[xc_from(g)], hgs.at[i], hgr.at[i])
     mixed = dot_t(hall[...].reshape(128, Q), wo[...].reshape(256, Q)).astype(BF)
-    for h in range(2):
-        rsend[h] = mixed[:, 128 * h : 128 * h + 128].reshape(XC, 16, 128)
-    rrecv[y, me] = rsend[y // 2, me]
+    rsend[...] = mixed.reshape(XC, 16, 256)
+    rrecv[y, me] = rsend[me]
     for i, (g, dy) in enumerate(pairs):
         if i:
             send(
-                rsend.at[yi(dy) // 2, xc_to(g)],
+                rsend.at[xc_to(g)],
                 rrecv.at[y, me],
                 rss.at[i],
                 rsr.at[i],
@@ -477,25 +481,23 @@
     for i, (g, dy) in enumerate(pairs):
         if i:
             arrive(rrecv.at[yi(-dy), xc_from(g)], rss.at[i], rsr.at[i])
-    sums = []
+    squares = jnp.zeros((16, 256), F32)
+    padding = iota((16, 256), 1) % 16 >= COLS
     for e in range(XC):
         total = rrecv[0, e].astype(F32)
         for k in range(1, NY):
             total = total + rrecv[k, e].astype(F32)
-        sums.append(total)
-    total = jnp.concatenate(sums, axis=1)
+        total = jnp.where(padding, 0.0, total)
+        after = (res_p[e] + total).astype(BF).astype(F32)
+        squares = squares + after * after
+        sum_s[e] = total
+    square = jnp.sum(squares, axis=-1, keepdims=True)
+    half = pl.ds(pl.multiple_of(128 * (y // 2), 128), 128)
+    total = jnp.concatenate([sum_s[e, :, half] for e in range(XC)], axis=1)
     both = dot(jnp.concatenate(split_two(total), axis=0), order_out[...])
     after = (res_s[:, own] + (both[0:16] + both[16:32])).astype(BF).astype(F32)
-    square = jnp.sum(after * after, axis=-1, keepdims=True)
-    ssend[...] = jnp.broadcast_to(square, (16, 128))
-    srecv[y] = ssend[...]
-    for k in range(1, NY):
-        send(ssend, srecv.at[y], sss.at[k], ssr.at[k], dev(dy=k))
     gained = after * ffn_gain
-    for k in range(1, NY):
-        arrive(srecv.at[yi(-k)], sss.at[k], ssr.at[k])
-    square = srecv[0] + srecv[1] + srecv[2] + srecv[3]
-    inverse = lax.rsqrt(square[:, 0:1] * (1.0 / D) + EPS)
+    inverse = lax.rsqrt(square * (1.0 / D) + EPS)
     tz[z] = (gained * inverse).astype(BF)
 
     quick_start(tok_ways)
@@ -553,6 +555,8 @@
 
     send(hf.at[y], hf.at[y], hs.at[0], hr.at[0], dev(dy=1))
     send(hf.at[y], hf.at[y], hs.at[1], hr.at[1], dev(dy=-1))
+    send(hf.at[y, pl.ds(0, 128)], hf.at[y, pl.ds(0, 128)], hs.at[2], hr.at[2], dev(dy=2))
+    send(hf.at[y, pl.ds(128, 128)], hf.at[y, pl.ds(128, 128)], hs.at[3], hr.at[3], dev(dy=-2))
     own_down.wait()
     for k in range(1, NY):
         arrive(dq.at[yi(-k)], ds_.at[k], dr.at[k])
@@ -561,9 +565,7 @@
     left = hf.at[yi(-1)]
     right = hf.at[yi(1)]
     arrive(left, hs.at[0], hr.at[0])
-    send(left.at[top], left.at[top], hs.at[2], hr.at[2], dev(dy=1))
     arrive(right, hs.at[1], hr.at[1])
-    send(right.at[bottom], right.at[bottom], hs.at[3], hr.at[3], dev(dy=-1))
     down = down + dot(hf[yi(-1)], dq[yi(-1)]) + dot(hf[yi(1)], dq[yi(1)])
     far = hf.at[yi(2)]
     arrive(far.at[top], hs.at[2], hr.at[2])
@@ -572,23 +574,41 @@
     osend[...] = down.astype(BF).reshape(XC, 32, Q)
 
     orecv[me] = osend[me]
-    for i, g in enumerate(groups[1:], 1):
-        send(osend.at[xc_to(g)], orecv.at[me], os_.at[i], or_.at[i], dev(dx=g[0], dc=g[1]))
+    parts = [pl.ds(0, Q)]
+    for f, part in enumerate(parts):
+        for i, g in enumerate(groups[1:], 1):
+            send(
+                osend.at[xc_to(g), :, part],
+                orecv.at[me, :, part],
+                os_.at[f, i],
+                or_.at[f, i],
+                dev(dx=g[0], dc=g[1]),
+            )
     to_z, to_e = r_id // 16, r_id % 16
     source = (to_e // 2) * 32 + (to_e % 2) * 16 + to_z
     turn = jnp.where(l_id == source, 1.0, 0.0).astype(BF)
-    for i, g in enumerate(groups[1:], 1):
-        arrive(orecv.at[xc_from(g)], os_.at[i], or_.at[i])
-    zsend[...] = dot(turn, orecv[...].reshape(256, Q)).astype(BF).reshape(NZ, 16, Q)
+    for f, part in enumerate(parts):
+        for i, g in enumerate(groups[1:], 1):
+            arrive(orecv.at[xc_from(g), :, part], os_.at[f, i], or_.at[f, i])
+        turned = dot(turn, orecv[:, :, 0:Q].reshape(256, Q))
+        zsend[:, :, 0:Q] = turned.astype(BF).reshape(NZ, 16, Q)
+        for d in (8, 7, 9, 6, 10, 5, 11, 4, 12, 3, 13, 2, 14, 1, 15):
+            send(
+                zsend.at[zi(d), :, part],
+                zrecv.at[z, :, part],
+                rets.at[f, d],
+                retr.at[f, d],
+                dev(dz=d),
+            )
     zrecv[z] = zsend[z]
-    for d in (8, 7, 9, 6, 10, 5, 11, 4, 12, 3, 13, 2, 14, 1, 15):
-        send(zsend.at[zi(d)], zrecv.at[z], rets.at[d], retr.at[d], dev(dz=d))
-    for d in range(1, NZ):
-        arrive(zrecv.at[zi(-d)], rets.at[d], retr.at[d])
-    back = zrecv[...].reshape(256, Q)
-    both = dot(jnp.concatenate([comb_hi, comb_lo], axis=0), back)
-    result = (after + (both[0:16] + both[16:32])).astype(BF)
-    out_ref[...] = result[0:SEQ, :]
+    comb = jnp.concatenate([comb_hi, comb_lo], axis=0)
+    for f, part in enumerate(parts):
+        for d in range(1, NZ):
+            arrive(zrecv.at[zi(-d), :, part], rets.at[f, d], retr.at[f, d])
+        span = slice(0, Q)
+        both = dot(comb, zrecv[:, :, span].reshape(256, Q))
+        result = (after[:, span] + (both[0:16] + both[16:32])).astype(BF)
+        out_ref[:, span] = result[0:SEQ, :]
     store.wait()
     for copy in pending:
         copy.wait_send()
@@ -648,10 +668,10 @@
             pltpu.VMEM((HL, 16, HEAD), F32),
             pltpu.VMEM((HL, 16, HEAD), F32),
             pltpu.VMEM((16, Q), BF),
-            pltpu.VMEM((2, XC, 16, 128), BF),
-            pltpu.VMEM((NY, XC, 16, 128), BF),
-            pltpu.VMEM((16, 128), F32),
-            pltpu.VMEM((NY, 16, 128), F32),
+            pltpu.VMEM((XC, 16, 256), BF),
+            pltpu.VMEM((NY, XC, 16, 256), BF),
+            pltpu.VMEM((XC, 16, 256), F32),
+            pltpu.VMEM((XC, 16, 256), F32),
             pltpu.VMEM((16, D), F32),
             pltpu.VMEM((128, 128), F32),
             pltpu.VMEM((128, 128), F32),
@@ -669,10 +689,11 @@
         ]
         + [
             dma((n,))
-            for n in (16, 16, 8, 8, 32, 32, 8, 8, 16, 16, 32, 32, 4, 4, 16, 16, 8, 8)
+            for n in (16, 16, 8, 8, 32, 32, 8, 8, 16, 16, 32, 32, 16, 16, 8, 8)
         ]
         + [dma((3, 8)), dma((3, 8))]
-        + [dma((n,)) for n in (4, 4, 4, 4, 8, 8, 16, 16, 20)],
+        + [dma((n,)) for n in (4, 4, 4, 4)]
+        + [dma((3, 8)), dma((3, 8)), dma((3, 16)), dma((3, 16)), dma((20,))],
         compiler_params=pltpu.CompilerParams(
             collective_id=0, has_side_effects=True, vmem_limit_bytes=60 * 1024 * 1024
         ),

time: 106 us -> 102 us (0.962)
  the two profiles are of different devices: /device:TPU:8 before, /device:TPU:1 now
where the time goes in v5:
time: 102 us
  Pallas kernels  99.9 us (98%)
  local copies, waits for them, and re-layouts  1.71 us (2%)
    pallas_call x1, Pallas kernels, shards(): pl.pallas_call(kernel, out_shape=(pltpu.VMEM((SEQ, Q), BF), pltpu.VMEM(re...  99.9 us

profile of v5, /device:TPU:1, one launch (start us, length us, event | category | flops | bytes accessed | tf_op | source)
XLA Modules:
  0.0 102.3 jit_solution(2667303130251460905)
XLA Ops:
  0.6 99.9 %shard_map.167 = (bf16[15,384]{1,0:T(8,128)(2,1)S(1)}, bf16[15,3,128,128]{3,2,1,0:T(8,128)(2,1)S(1)}) custom-call(bf16[15,1536]{1,0:T(8,128)(2,1)} %res_hbm.1, bf16[12,384]{1,0:T(8,128)(2,1)} %bitcast.13, bf16[12,384]{1,0:T(8,128)(2,1)} %bitcast.14, bf16[12,384]{1,0:T(8,128)(2,1)} %bitcast.15, bf16[12,384]{1,0:T(8,128)(2,1)} %bitcast.16, ...), custom_call_target="tpu_custom_call" | custom-call | tf_op jit(solution)/shard_map/pallas_call | solution.py:639
  100.6 0.6 copy.20
  101.2 1.1 %copy.21 = bf16[15,3,128,128]{3,2,1,0:T(8,128)(2,1)} copy(bf16[15,3,128,128]{3,2,1,0:T(8,128)(2,1)S(1)} %get-tuple-element.3) | data formatting | bytes 2949120
